TPU v7x, 256 devices: a whole 4x4x8 slice. The times are simulated.
256 devices in a mesh: dp: 4 (over y), kv: 32 (over z, x), tp: 2 (over core).
Axes of the slice: x: 4, y: 4, z: 8, core: 2. Of those that a mesh axis runs over, the one named last changes fastest.
Arguments:
- tokens: bfloat16 [16, 16, 2048], P('dp', None, 'kv'), may hold values from -6 to 6
- norm_gain: float32 [2048], P('kv'), may hold values from 0.1 to 1.9
- w_query: bfloat16 [2048, 1024], P('kv', 'tp'), may hold values from -0.125 to 0.125
- w_key: bfloat16 [2048, 1024], P('kv', 'tp'), may hold values from -0.125 to 0.125
- w_value: bfloat16 [2048, 1024], P('kv', 'tp'), may hold values from -0.125 to 0.125
- w_forget: bfloat16 [2048, 16], replicated, may hold values from -0.125 to 0.125
- forget_bias: float32 [16], replicated, may hold values from -2 to 4
- query_gain: float32 [64], replicated, may hold values from 0.1 to 1.9
- key_gain: float32 [64], replicated, may hold values from 0.1 to 1.9
- head_gain: float32 [64], replicated, may hold values from 0.1 to 1.9
- w_out: bfloat16 [1024, 2048], P('tp', 'kv'), may hold values from -0.1875 to 0.1875
- key_cache: bfloat16 [16, 16384, 1024], P('dp', 'kv', 'tp'), may hold values from -240 to 240
- value_cache: bfloat16 [16, 16384, 1024], P('dp', 'kv', 'tp'), may hold values from -6 to 6
- gate_cache: float32 [16, 16, 16384], P('dp', 'tp', 'kv'), may hold values from -1922 to 0, as said below
- lengths: int32 [16], P('dp'), may hold values from 15341 to 16364
- accepted: int32 [16], P('dp'), may hold values from 0 to 4
- parents: int32 [16, 16], P('dp'), may hold values from -1 to 14, as said below
Outputs:
- layer_out: bfloat16 [16, 16, 2048], P('dp', None, 'kv')
- new_keys: bfloat16 [16, 16384, 1024], P('dp', 'kv', 'tp')
- new_values: bfloat16 [16, 16384, 1024], P('dp', 'kv', 'tp')
- proposal_gates: float32 [16, 16, 16], P('dp', None, 'tp')
Inputs may be any that keep to these rules, and one draw needn't show every extreme that they name: `gate_cache`: each entry is the running sum of log forget gates up to its position, so entries never rise along positions; entries at and after lengths hold the last step's proposals in order. `parents`: proposal 0 follows the last accepted token (parent -1); every other proposal's parent is one of the three proposals before it.
All inputs are finite; a program needn't handle non-finite values.
Results may differ from a plain program's by a relative error of at most 0.0051.
The roundings to bfloat16 on the way count: a program that leaves them out, or rounds other values in their place, can miss the bound.
Values may be sent and summed in bfloat16 or wider, within the bound.
A program may use at most 64 MiB of HBM per device.

v0:
```python
import jax
import jax.numpy as jnp
from jax import lax
from jax.sharding import PartitionSpec as P

EPSILON = 1e-06
MASKED = -1e30


def padded_to(lines, devices):
    spare = -lines.shape[0] % devices
    if not spare:
        return lines
    return jnp.concatenate([lines, jnp.zeros((spare, *lines.shape[1:]), lines.dtype)])


def from_everyone(array, axis):
    devices = lax.axis_size(axis)
    return lax.all_to_all(
        jnp.broadcast_to(array[None], (devices, *array.shape)), axis, 0, 0, tiled=True
    )


def joined_along(parts, dim):
    parts = jnp.moveaxis(parts, 0, dim)
    lengths = parts.shape
    return parts.reshape(*lengths[:dim], lengths[dim] * lengths[dim + 1], *lengths[dim + 2 :])


def collect(array, axis, dim):
    parts = from_everyone(array, axis)
    return joined_along(parts, dim)


def cut_along(array, dim, devices):
    before, after = (array.shape[:dim], array.shape[dim + 1 :])
    return jnp.moveaxis(array.reshape(*before, devices, -1, *after), dim, 0)


def summed_on_arrival(array, axis, dim):
    parts = cut_along(array, dim, lax.axis_size(axis))
    arrived = lax.all_to_all(parts, axis, split_axis=0, concat_axis=0, tiled=True)
    return arrived.sum(axis=0)


def total_of(array, axes):
    padded = padded_to(array, lax.axis_size(axes))
    whole = collect(summed_on_arrival(padded, axes, 0), axes, 0)
    return lax.slice_in_dim(whole, 0, len(array)).reshape(array.shape)


def packed_total(arrays, axis):
    ends = [0]
    for a in arrays:
        ends.append(ends[-1] + a.size)
    total = total_of(jnp.concatenate([a.ravel() for a in arrays]), axis)
    return tuple((total[b:e].reshape(a.shape) for a, b, e in zip(arrays, ends, ends[1:])))


def of_everyone(array, axis):
    return from_everyone(array, axis).astype(jnp.float32).sum(axis=0)


def head_norm(head_rows, gain_vec):
    mean_square = jnp.mean(head_rows * head_rows, axis=-1, keepdims=True)
    return head_rows * lax.rsqrt(mean_square + EPSILON) * gain_vec


def ancestry(parents):
    count_all = parents.shape[1]
    step_ids = jnp.arange(count_all, dtype=jnp.int32)
    step_matrix = (parents[:, :, None] == step_ids[None, None, :]).astype(jnp.float32)
    identity = jnp.broadcast_to(jnp.eye(count_all, dtype=jnp.float32), step_matrix.shape)

    def extend(turn_index, ancestors):
        return identity + jnp.einsum(
            "sij,sjk->sik", step_matrix, ancestors, precision=lax.Precision.HIGHEST
        )

    return lax.fori_loop(0, count_all, extend, identity)


def combine(earlier, later):
    earlier_max, earlier_total, earlier_sum = earlier
    later_max, later_total, later_sum = later
    row_max = jnp.maximum(earlier_max, later_max)
    earlier_scale = jnp.exp(earlier_max - row_max)
    later_scale = jnp.exp(later_max - row_max)
    spread = earlier_max.shape + (-1,)
    joined = (
        earlier_sum.reshape(spread) * earlier_scale[..., None]
        + later_sum.reshape(spread) * later_scale[..., None]
    )
    return (
        row_max,
        earlier_total * earlier_scale + later_total * later_scale,
        joined.reshape(earlier_sum.shape),
    )


def block_part(scores, live_mask, block_values):
    seq_count, heads_local, prop_count, key_count = scores.shape
    row_max = jnp.max(scores, axis=3)
    weights = jnp.where(live_mask, jnp.exp(scores - row_max[..., None]), 0.0)
    row_total = jnp.sum(weights, axis=3)
    weighted = jnp.einsum(
        "shpk,skhd->sphd",
        weights.astype(jnp.bfloat16),
        block_values,
        preferred_element_type=jnp.float32,
    )
    return (
        jnp.transpose(row_max, (0, 2, 1)),
        jnp.transpose(row_total, (0, 2, 1)),
        weighted.reshape(seq_count, prop_count, -1),
    )


def finish_rows(row_sums, inverse, query_gain, key_gain, heads_local):
    head_width = row_sums.shape[1] // 3
    head_size = head_width // heads_local
    row_count = row_sums.shape[0]
    raw_sums = row_sums * inverse[:, None]
    queries = head_norm(
        raw_sums[:, :head_width].reshape(row_count, heads_local, head_size), query_gain
    )
    keyed = head_norm(
        raw_sums[:, head_width : 2 * head_width].reshape(row_count, heads_local, head_size),
        key_gain,
    )
    return jnp.concatenate(
        [
            queries.reshape(row_count, head_width),
            keyed.reshape(row_count, head_width),
            raw_sums[:, 2 * head_width :],
        ],
        axis=1,
    ).astype(jnp.bfloat16)


def flatten_part(part_triple, rows_all):
    part_max, part_total, part_sum = part_triple
    return (
        part_max.reshape(rows_all, -1),
        part_total.reshape(rows_all, -1),
        part_sum.reshape(rows_all, -1),
    )


def shards(
    tokens,
    norm_gain,
    w_query,
    w_key,
    w_value,
    w_forget,
    forget_bias,
    query_gain,
    key_gain,
    head_gain,
    w_out,
    key_cache,
    value_cache,
    gate_cache,
    lengths,
    accepted,
    parents,
):
    seq_count, prop_count, width_in = tokens.shape
    pos_dev = key_cache.shape[1]
    heads_local = gate_cache.shape[1]
    head_width = key_cache.shape[2]
    head_size = head_width // heads_local
    rows_all = seq_count * prop_count
    full_width = w_forget.shape[0]
    kv_index = lax.axis_index("kv")
    tp_index = lax.axis_index("tp")
    flattened = tokens.reshape(rows_all, width_in).astype(jnp.float32)
    squares = jnp.sum(flattened * flattened, axis=1)
    scaled = (flattened * norm_gain).astype(jnp.bfloat16)
    w_rows = lax.dynamic_slice_in_dim(w_forget, kv_index * width_in, width_in, 0)
    gate_part = jnp.dot(scaled, w_rows, preferred_element_type=jnp.float32)
    w_joined = jnp.concatenate([w_query, w_key, w_value], axis=1)
    summed, gate_sum, square_sum = packed_total(
        (jnp.dot(scaled, w_joined, preferred_element_type=jnp.float32), gate_part, squares), "kv"
    )
    inverse = lax.rsqrt(square_sum / full_width + EPSILON)
    joined = finish_rows(summed, inverse, query_gain, key_gain, heads_local)
    log_all = jax.nn.log_sigmoid(gate_sum * inverse[:, None] + forget_bias)
    log_own = lax.dynamic_slice_in_dim(log_all, tp_index * heads_local, heads_local, 1)
    log_own = log_own.reshape(seq_count, prop_count, heads_local)
    queries = joined[:, :head_width].reshape(seq_count, prop_count, heads_local, head_size)
    keys_new = joined[:, head_width : 2 * head_width].reshape(
        seq_count, prop_count, heads_local, head_size
    )
    values_new = joined[:, 2 * head_width :].reshape(seq_count, prop_count, heads_local, head_size)
    ancestors = ancestry(parents)
    path_sum = jnp.einsum("sij,sjh->sih", ancestors, log_own, precision=lax.Precision.HIGHEST)
    base_pos = lengths + accepted
    positions = kv_index * pos_dev + jnp.arange(pos_dev, dtype=jnp.int32)
    score_scale = head_size ** (-0.5)
    cached_keys = key_cache.reshape(seq_count, pos_dev, heads_local, head_size)
    cached_values = value_cache.reshape(seq_count, pos_dev, heads_local, head_size)
    scores = jnp.einsum("sphd,skhd->shpk", queries, cached_keys, preferred_element_type=jnp.float32)
    scores = scores * score_scale - gate_cache[:, :, None, :]
    live_mask = (positions[None, :] < base_pos[:, None])[:, None, None, :]
    scores = jnp.where(live_mask, scores, MASKED)
    local_part = block_part(scores, live_mask, cached_values)
    hit_mask = positions[None, :] == (base_pos - 1)[:, None]
    boundary_local = jnp.sum(jnp.where(hit_mask[:, None, :], gate_cache, 0.0), axis=2)
    tree_live = (ancestors > 0.5)[:, None, :, :]
    owner_mask = jnp.any(hit_mask, axis=1)
    tree_scores = jnp.einsum(
        "sphd,sjhd->shpj", queries, keys_new, preferred_element_type=jnp.float32
    )
    tree_scores = (
        tree_scores * score_scale
        - jnp.transpose(path_sum, (0, 2, 1))[:, :, None, :]
        - boundary_local[:, :, None, None]
    )
    tree_scores = jnp.where(tree_live, tree_scores, MASKED)
    tree_max, tree_total, tree_sum = block_part(tree_scores, tree_live, values_new)
    tree_max = jnp.where(owner_mask[:, None, None], tree_max, MASKED)
    tree_total = jnp.where(owner_mask[:, None, None], tree_total, 0.0)
    tree_sum = jnp.where(owner_mask[:, None, None], tree_sum, 0.0)
    partial_value = combine(local_part, (tree_max, tree_total, tree_sum))
    flat_max, flat_total, flat_sum = flatten_part(partial_value, rows_all)
    got_max, got_total, got_sum = (
        lax.all_to_all(flat_max[None], "kv", split_axis=1, concat_axis=0, tiled=True),
        lax.all_to_all(flat_total[None], "kv", split_axis=1, concat_axis=0, tiled=True),
        lax.all_to_all(flat_sum[None], "kv", split_axis=1, concat_axis=0, tiled=True),
    )
    top = jnp.max(got_max, axis=0)
    factors = jnp.exp(got_max - top[None])
    own_rows = got_max.shape[1]
    summed_rows = jnp.sum(
        got_sum.reshape(got_sum.shape[0], own_rows, heads_local, head_size) * factors[..., None],
        axis=0,
    )
    merged = (top, jnp.sum(got_total * factors, axis=0), summed_rows.reshape(own_rows, head_width))
    row_max, row_total, weighted = merged
    attended = weighted.reshape(own_rows, heads_local, head_size) / row_total[..., None]
    own_normed = head_norm(attended, head_gain).astype(jnp.bfloat16).reshape(own_rows, head_width)
    normed = collect(own_normed, "kv", 0)
    out_term = jnp.dot(normed, w_out, preferred_element_type=jnp.float32)
    layer_out = (
        of_everyone(out_term.astype(jnp.bfloat16), "tp").astype(jnp.float32).astype(jnp.bfloat16)
    )
    layer_out = layer_out.reshape(seq_count, prop_count, -1)
    new_rows = jnp.concatenate(
        [
            keys_new.reshape(seq_count, prop_count, head_width),
            values_new.reshape(seq_count, prop_count, head_width),
        ],
        axis=2,
    )
    slot_index = positions[None, :, None] - base_pos[:, None, None]
    placing = slot_index == jnp.arange(prop_count, dtype=jnp.int32)[None, None, :]
    written = jnp.einsum(
        "skp,spc->skc", placing.astype(jnp.bfloat16), new_rows, preferred_element_type=jnp.float32
    ).astype(jnp.bfloat16)
    hit_rows = jnp.any(placing, axis=2)[..., None]
    new_keys = jnp.where(hit_rows, written[..., :head_width], key_cache)
    new_values = jnp.where(hit_rows, written[..., head_width:], value_cache)
    return (layer_out, new_keys, new_values, log_own)


def solution(mesh):
    placed = (
        P("dp", None, "kv"),
        P("kv"),
        P("kv", "tp"),
        P("kv", "tp"),
        P("kv", "tp"),
        P(),
        P(),
        P(),
        P(),
        P(),
        P("tp", "kv"),
        P("dp", "kv", "tp"),
        P("dp", "kv", "tp"),
        P("dp", "tp", "kv"),
        P("dp"),
        P("dp"),
        P("dp", None),
    )
    return jax.shard_map(
        shards,
        mesh=mesh,
        in_specs=placed,
        out_specs=(
            P("dp", None, "kv"),
            P("dp", "kv", "tp"),
            P("dp", "kv", "tp"),
            P("dp", None, "tp"),
        ),
        check_vma=False,
    )
```

profile of v0, /device:TPU:1, one launch (start us, length us, event | category | flops | bytes accessed | tf_op | source)
XLA Modules:
  0.0 130.6 jit_solution(2430243420172668842)
XLA Ops:
  0.7 0.8 multiply_reduce_fusion.2
  1.6 0.7 fusion.48
  2.3 0.9 fusion.53
  3.3 1.1 fusion.23
  4.5 1.3 %all_to_all.43 = f32[32,1,3106]{2,1,0:T(1,128)} reshape(f32[99392]{0:T(1024)S(1)} %pad_maximum_fusion) | data formatting | bytes 795136 | tf_op jit(solution)/shard_map/all_to_all | solution.py:42
  5.8 11.9 %all-to-all-start = ((f32[32,1,3106]{2,1,0:T(1,128)}), f32[32,1,3106]{2,1,0:T(1,128)S(1)}, u32[]{:S(2)}, u32[]{:S(2)}) async-start(f32[32,1,3106]{2,1,0:T(1,128)} %all_to_all.43), calls=%async_computation | async-start | bytes 819200 | tf_op jit(solution)/shard_map/all_to_all | solution.py:42
  17.7 4.2 %while.11 = (s32[]{:T(128)}, f32[4,16,16]{2,1,0:T(8,128)S(1)}, s32[4,16]{1,0:T(4,128)S(1)}, f32[16,16]{1,0:T(8,128)S(1)}, s32[]{:T(128)}) while((s32[]{:T(128)}, f32[4,16,16]{2,1,0:T(8,128)S(1)}, s32[4,16]{1,0:T(4,128)S(1)}, f32[16,16]{1,0:T(8,128)S(1)}, s32[]{:T(128)}) %tuple.48), condition=%wide.region_6.7_spmd.clone, body=%wide.region_5.6_spmd.clone.sunk | while | flops 199682 | bytes 17725 | solution.py:80
  17.7 0.2 convolution_add_fusion.2
  18.0 0.2 convolution_add_fusion.2
  18.3 0.2 convolution_add_fusion.2
  18.5 0.2 convolution_add_fusion.2
  18.8 0.2 convolution_add_fusion.2
  19.1 0.2 convolution_add_fusion.2
  19.3 0.2 convolution_add_fusion.2
  19.6 0.2 convolution_add_fusion.2
  19.8 0.2 convolution_add_fusion.2
  20.1 0.2 convolution_add_fusion.2
  20.4 0.2 convolution_add_fusion.2
  20.6 0.2 convolution_add_fusion.2
  20.9 0.2 convolution_add_fusion.2
  21.2 0.2 convolution_add_fusion.2
  21.4 0.2 convolution_add_fusion.2
  21.7 0.2 convolution_add_fusion.2
  22.1 0.6 mul.237
  22.9 2.4 %copy.142 = bf16[4,512,512]{1,2,0:T(8,128)(2,1)} copy(bf16[4,512,512]{2,1,0:T(8,128)(2,1)S(1)} %copy-done.2) | data formatting | bytes 4194304 | tf_op args[11]
  25.3 2.8 %copy.144 = bf16[4,512,512]{1,2,0:T(8,128)(2,1)S(1)} copy(bf16[4,512,512]{2,1,0:T(8,128)(2,1)} %param.31) | data formatting | bytes 4194304 | tf_op args[12]
  28.1 3.5 %all-to-all-done = f32[32,1,3106]{2,1,0:T(1,128)S(1)} async-done(((f32[32,1,3106]{2,1,0:T(1,128)}), f32[32,1,3106]{2,1,0:T(1,128)S(1)}, u32[]{:S(2)}, u32[]{:S(2)}) %all-to-all-start) | async-done | bytes 397600 | tf_op jit(solution)/shard_map/all_to_all | solution.py:42
  31.6 0.2 reduce_sum.108
  31.9 1.0 broadcast_in_dim.148
  32.8 5.7 %all-to-all-start.1 = ((f32[32,1,3106]{2,1,0:T(1,128)}), f32[32,1,3106]{2,1,0:T(1,128)S(1)}, u32[]{:S(2)}, u32[]{:S(2)}) async-start(f32[32,1,3106]{2,1,0:T(1,128)} %broadcast_in_dim.148), calls=%async_computation.1 | async-start | bytes 819200 | tf_op jit(solution)/shard_map/all_to_all | solution.py:19
  38.7 0.6 fusion.35
  39.3 1.3 fusion.64
  40.6 0.7 select_reduce_fusion
  41.3 10.9 %all-to-all-done.1 = f32[32,1,3106]{2,1,0:T(1,128)S(1)} async-done(((f32[32,1,3106]{2,1,0:T(1,128)}), f32[32,1,3106]{2,1,0:T(1,128)S(1)}, u32[]{:S(2)}, u32[]{:S(2)}) %all-to-all-start.1) | async-done | bytes 397600 | tf_op jit(solution)/shard_map/all_to_all | solution.py:19
  52.1 1.0 reduce.4
  53.4 3.5 %slice.41 = f32[6212,16]{1,0:T(8,128)} reshape(f32[32,3106]{1,0:T(8,128)S(1)} %reduce.4) | data formatting | bytes 795136 | tf_op jit(solution)/shard_map/slice | solution.py:57
  58.7 0.8 reshape.283
  59.4 0.8 fusion.65
  60.6 2.1 %fusion.67 = (f32[4,8,16]{2,1,0:T(8,128)S(1)}, f32[4,8,16,512]{3,2,1,0:T(8,128)S(1)}) fusion(f32[4,8,512]{2,1,0:T(8,128)S(1)} %copy-done.7, bf16[4,512,8,64]{1,3,2,0:T(8,128)(2,1)} %bitcast.63, bf16[4,16,8,64]{3,2,1,0:T(8,128)(2,1)S(1)} %reshape.280, pred[4,512]{1,0:T(4,128)(4,1)S(1)} %copy-done.14), kind=kOutput, calls=%fused_computation.107 | convolution fusion | flops 34602496 | bytes 3280896 | tf_op jit(solution)/shard_map/sphd,skhd->shpk/dot_general | solution.py:204
  62.8 0.3 fusion.15
  63.1 0.2 fusion.68
  63.4 0.7 copy-done.4
  64.2 0.7 fusion.49
  64.9 0.7 copy.166
  65.6 5.6 %all-to-all-start.4 = ((f32[1,64,8]{2,0,1:T(1,128)}), f32[1,64,8]{2,0,1:T(1,128)}, u32[]{:S(2)}, u32[]{:S(2)}) async-start(f32[1,64,8]{2,0,1:T(1,128)} %bitcast.13), calls=%async_computation.4 | async-start | bytes 65536 | tf_op jit(solution)/shard_map/all_to_all | solution.py:230
  71.2 1.4 %fusion.13 = f32[4,16,8,64]{3,1,2,0:T(8,128)S(1)} fusion(bf16[4,512,8,64]{1,3,2,0:T(8,128)(2,1)S(1)} %bitcast.62, f32[4,8,16,512]{3,2,1,0:T(8,128)S(1)} %get-tuple-element.96, f32[4,8,16]{2,1,0:T(8,128)S(1)} %get-tuple-element.95, pred[4,512]{1,0:T(4,128)(4,1)} %get-tuple-element.94, f32[4,16,8]{1,2,0:T(8,128)} %get-tuple-element.80), kind=kOutput, calls=%fused_computation.20 | convolution fusion | flops 34373632 | bytes 3282944 | tf_op jit(solution)/shard_map/shpk,skhd->sphd/dot_general | solution.py:106
  72.6 0.9 slice.73
  73.7 1.4 %copy.165 = f32[4,16,8]{2,1,0:T(8,128)} copy(f32[4,16,8]{1,2,0:T(8,128)} %get-tuple-element.81) | data formatting | bytes 4096 | tf_op jit(solution)/shard_map/broadcast_in_dim;reshape | solution.py:229
  75.1 4.7 %all-to-all-done.4 = f32[1,64,8]{2,0,1:T(1,128)} async-done(((f32[1,64,8]{2,0,1:T(1,128)}), f32[1,64,8]{2,0,1:T(1,128)}, u32[]{:S(2)}, u32[]{:S(2)}) %all-to-all-start.4) | async-done | bytes 2080 | tf_op jit(solution)/shard_map/all_to_all | solution.py:230
  79.8 4.4 %all-to-all-start.3 = ((f32[1,64,8]{2,0,1:T(1,128)}), f32[1,64,8]{2,0,1:T(1,128)S(1)}, u32[]{:S(2)}, u32[]{:S(2)}) async-start(f32[1,64,8]{2,0,1:T(1,128)} %bitcast.9), calls=%async_computation.3 | async-start | bytes 65536 | tf_op jit(solution)/shard_map/all_to_all | solution.py:229
  84.2 1.2 fusion.10
  85.6 0.8 broadcast_in_dim_reshape_reshape.4
  86.4 6.5 %all-to-all-done.3 = f32[1,64,8]{2,0,1:T(1,128)S(1)} async-done(((f32[1,64,8]{2,0,1:T(1,128)}), f32[1,64,8]{2,0,1:T(1,128)S(1)}, u32[]{:S(2)}, u32[]{:S(2)}) %all-to-all-start.3) | async-done | bytes 2080 | tf_op jit(solution)/shard_map/all_to_all | solution.py:229
  92.9 4.0 %all-to-all-start.2 = ((f32[1,64,512]{2,0,1:T(1,128)}), f32[1,64,512]{2,0,1:T(1,128)S(1)}, u32[]{:S(2)}, u32[]{:S(2)}) async-start(f32[1,64,512]{2,0,1:T(1,128)} %broadcast_in_dim_reshape_reshape.4), calls=%async_computation.2 | async-start | bytes 262144 | tf_op jit(solution)/shard_map/all_to_all | solution.py:231
  97.0 3.2 %convolution_convert_fusion = bf16[4,512,1024]{2,1,0:T(8,128)(2,1)} fusion(bf16[4,16,512]{2,1,0:T(8,128)(2,1)S(1)} %bitcast.65, bf16[4,16,512]{2,1,0:T(8,128)(2,1)S(1)} %bitcast.64, s32[4,512]{1,0:T(4,128)S(1)} %copy-done.12), kind=kOutput, calls=%fused_computation.6 | convolution fusion | flops 69500928 | bytes 4333568 | tf_op jit(solution)/shard_map/skp,spc->skc/dot_general | solution.py:259
  100.3 0.8 multiply_reduce_fusion.1
  101.6 4.6 %all-to-all-done.2 = f32[1,64,512]{2,0,1:T(1,128)S(1)} async-done(((f32[1,64,512]{2,0,1:T(1,128)}), f32[1,64,512]{2,0,1:T(1,128)S(1)}, u32[]{:S(2)}, u32[]{:S(2)}) %all-to-all-start.2) | async-done | bytes 131104 | tf_op jit(solution)/shard_map/all_to_all | solution.py:231
  106.8 0.7 broadcast_in_dim.162
  107.5 4.4 %all-to-all-start.5 = ((bf16[32,2,512]{2,1,0:T(2,128)(2,1)}), bf16[32,2,512]{2,1,0:T(2,128)(2,1)S(1)}, u32[]{:S(2)}, u32[]{:S(2)}) async-start(bf16[32,2,512]{2,1,0:T(2,128)(2,1)} %broadcast_in_dim.162), calls=%async_computation.5 | async-start | bytes 131072 | tf_op jit(solution)/shard_map/all_to_all | solution.py:19
  111.9 4.4 %slice_select_fusion = (bf16[4,512,512]{2,1,0:T(8,128)(2,1)}, bf16[4,512,512]{2,1,0:T(8,128)(2,1)}) fusion(bf16[4,512,512]{2,1,0:T(8,128)(2,1)S(1)} %copy-done.1, bf16[4,512,1024]{2,1,0:T(8,128)(2,1)} %convolution_convert_fusion, pred[4,512]{1,0:T(4,128)(4,1)S(1)} %copy-done.16, bf16[4,512,512]{2,1,0:T(8,128)(2,1)} %param.30), kind=kLoop, calls=%fused_computation.7 | loop fusion | flops 2097152 | bytes 12584960 | tf_op jit(solution)/shard_map/jit(_where)/select_n | solution.py:264
  116.4 0.7 copy.151
  117.1 3.7 %all-to-all-done.5 = bf16[32,2,512]{2,1,0:T(2,128)(2,1)S(1)} async-done(((bf16[32,2,512]{2,1,0:T(2,128)(2,1)}), bf16[32,2,512]{2,1,0:T(2,128)(2,1)S(1)}, u32[]{:S(2)}, u32[]{:S(2)}) %all-to-all-start.5) | async-done | bytes 65568 | tf_op jit(solution)/shard_map/all_to_all | solution.py:19
  121.0 8.8 %all_to_all.61 = bf16[2,2,2048]{2,1,0:T(2,128)(2,1)S(1)} all-to-all(bf16[2,2,2048]{2,1,0:T(2,128)(2,1)S(1)} %reshape.291), channel_id=1, replica_groups=mesh['dp'=4,'kv'=32,'tp'=2] {'tp'}, dimensions={0} | all-to-all | bytes 32768 | tf_op jit(solution)/shard_map/all_to_all | solution.py:19
  130.0 0.6 reduce_sum.118
  (125 shorter events, 4.7 us)
Async XLA Ops:
  0.6 120.1 %copy-start = (bf16[512,64]{0,1:T(8,128)(2,1)S(1)}, bf16[512,64]{0,1:T(8,128)(2,1)}, u32[]{:S(2)}) copy-start(bf16[512,64]{0,1:T(8,128)(2,1)} %param.29) | copy-start | bytes 196612
  0.6 17.1 %copy-start.13 = (s32[4,16]{1,0:T(4,128)S(1)}, s32[4,16]{1,0:T(4,128)}, u32[]{:S(2)}) copy-start(s32[4,16]{1,0:T(4,128)} %param.35) | copy-start | bytes 772
  4.4 17.6 %copy-start.20 = (f32[64]{0:T(128)S(1)}, f32[64]{0:T(128)}, u32[]{:S(2)}) copy-start(f32[64]{0:T(128)} %param.26) | copy-start | bytes 772
  4.4 17.7 %copy-start.21 = (f32[64]{0:T(128)S(1)}, f32[64]{0:T(128)}, u32[]{:S(2)}) copy-start(f32[64]{0:T(128)} %param.27) | copy-start | bytes 772
  4.4 17.7 %copy-start.22 = (f32[64]{0:T(128)S(1)}, f32[64]{0:T(128)}, u32[]{:S(2)}) copy-start(f32[64]{0:T(128)} %param.28) | copy-start | bytes 772
  4.4 18.5 %copy-start.2 = (bf16[4,512,512]{2,1,0:T(8,128)(2,1)S(1)}, bf16[4,512,512]{2,1,0:T(8,128)(2,1)}, u32[]{:S(2)}) copy-start(bf16[4,512,512]{2,1,0:T(8,128)(2,1)} %param.30) | copy-start | bytes 6291460
  5.8 25.8 %all-to-all-start = ((f32[32,1,3106]{2,1,0:T(1,128)}), f32[32,1,3106]{2,1,0:T(1,128)S(1)}, u32[]{:S(2)}, u32[]{:S(2)}) async-start(f32[32,1,3106]{2,1,0:T(1,128)} %all_to_all.43), calls=%async_computation | async-start | bytes 819200 | tf_op jit(solution)/shard_map/all_to_all | solution.py:42
  22.9 40.5 %copy-start.10 = (pred[4,16,16]{1,2,0:T(8,128)(4,1)}, pred[4,16,16]{1,2,0:T(8,128)(4,1)S(1)}, u32[]{:S(2)}) copy-start(pred[4,16,16]{1,2,0:T(8,128)(4,1)S(1)} %copy.145) | copy-start | bytes 3076
  25.3 2.8 %copy-start.23 = (s32[4]{0:T(128)S(1)}, s32[4]{0:T(128)}, u32[]{:S(2)}) copy-start(s32[4]{0:T(128)} %param.33) | copy-start | bytes 52
  25.3 2.8 %copy-start.24 = (s32[4]{0:T(128)S(1)}, s32[4]{0:T(128)}, u32[]{:S(2)}) copy-start(s32[4]{0:T(128)} %param.34) | copy-start | bytes 52
  25.3 15.3 %copy-start.7 = (f32[4,8,512]{2,1,0:T(8,128)S(1)}, f32[4,8,512]{2,1,0:T(8,128)}, u32[]{:S(2)}) copy-start(f32[4,8,512]{2,1,0:T(8,128)} %param.32) | copy-start | bytes 196612
  32.8 19.3 %all-to-all-start.1 = ((f32[32,1,3106]{2,1,0:T(1,128)}), f32[32,1,3106]{2,1,0:T(1,128)S(1)}, u32[]{:S(2)}, u32[]{:S(2)}) async-start(f32[32,1,3106]{2,1,0:T(1,128)} %broadcast_in_dim.148), calls=%async_computation.1 | async-start | bytes 819200 | tf_op jit(solution)/shard_map/all_to_all | solution.py:19
  38.7 14.7 %copy-start.11 = (s32[4,512]{1,0:T(4,128)}, s32[4,512]{1,0:T(4,128)S(1)}, u32[]{:S(2)}) copy-start(s32[4,512]{1,0:T(4,128)S(1)} %broadcast_subtract_fusion) | copy-start | bytes 24580
  57.1 1.6 %copy-start.3 = (f32[64,1536]{1,0:T(8,128)}, f32[64,1536]{1,0:T(8,128)S(1)}, u32[]{:S(2)}) copy-start(f32[64,1536]{1,0:T(8,128)S(1)} %broadcast_multiply_fusion) | copy-start | bytes 1179652
  57.1 2.3 %copy-start.19 = (f32[16]{0:T(128)S(1)}, f32[16]{0:T(128)}, u32[]{:S(2)}) copy-start(f32[16]{0:T(128)} %param.25) | copy-start | bytes 196
  57.1 3.5 %copy-start.14 = (pred[4,512]{1,0:T(4,128)(4,1)S(1)}, pred[4,512]{1,0:T(4,128)(4,1)}, u32[]{:S(2)}) copy-start(pred[4,512]{1,0:T(4,128)(4,1)} %get-tuple-element.94) | copy-start | bytes 6148
  60.4 2.7 %copy-start.5 = (f32[64,8]{1,0:T(8,128)}, f32[64,8]{1,0:T(8,128)S(1)}, u32[]{:S(2)}) copy-start(f32[64,8]{1,0:T(8,128)S(1)} %fusion.42) | copy-start | bytes 6148
  60.6 2.5 %copy-start.9 = (bf16[4,16,8,64]{3,2,1,0:T(8,128)(2,1)S(1)}, bf16[4,16,8,64]{3,2,1,0:T(8,128)(2,1)}, u32[]{:S(2)}) copy-start(bf16[4,16,8,64]{3,2,1,0:T(8,128)(2,1)} %reshape.283) | copy-start | bytes 196612
  60.6 2.5 %copy-start.18 = (f32[4,8]{1,0:T(4,128)S(1)}, f32[4,8]{1,0:T(4,128)}, u32[]{:S(2)}) copy-start(f32[4,8]{1,0:T(4,128)} %select_reduce_fusion) | copy-start | bytes 388
  60.6 3.5 %copy-start.17 = (pred[4]{0:T(512)(128)(4,1)S(1)}, pred[4]{0:T(512)(128)(4,1)}, u32[]{:S(2)}) copy-start(pred[4]{0:T(512)(128)(4,1)} %get-tuple-element.82) | copy-start | bytes 16
  63.4 0.7 copy-start.4
  63.4 7.8 %copy-start.8 = (f32[4,8,16]{2,1,0:T(8,128)}, f32[4,8,16]{2,1,0:T(8,128)S(1)}, u32[]{:S(2)}) copy-start(f32[4,8,16]{2,1,0:T(8,128)S(1)} %get-tuple-element.97) | copy-start | bytes 6148
  65.6 14.3 %all-to-all-start.4 = ((f32[1,64,8]{2,0,1:T(1,128)}), f32[1,64,8]{2,0,1:T(1,128)}, u32[]{:S(2)}, u32[]{:S(2)}) async-start(f32[1,64,8]{2,0,1:T(1,128)} %bitcast.13), calls=%async_computation.4 | async-start | bytes 65536 | tf_op jit(solution)/shard_map/all_to_all | solution.py:230
  72.6 24.4 %copy-start.12 = (s32[4,512]{1,0:T(4,128)S(1)}, s32[4,512]{1,0:T(4,128)}, u32[]{:S(2)}) copy-start(s32[4,512]{1,0:T(4,128)} %copy-done.11) | copy-start | bytes 24580
  79.8 13.1 %all-to-all-start.3 = ((f32[1,64,8]{2,0,1:T(1,128)}), f32[1,64,8]{2,0,1:T(1,128)S(1)}, u32[]{:S(2)}, u32[]{:S(2)}) async-start(f32[1,64,8]{2,0,1:T(1,128)} %bitcast.9), calls=%async_computation.3 | async-start | bytes 65536 | tf_op jit(solution)/shard_map/all_to_all | solution.py:229
  92.9 13.3 %all-to-all-start.2 = ((f32[1,64,512]{2,0,1:T(1,128)}), f32[1,64,512]{2,0,1:T(1,128)S(1)}, u32[]{:S(2)}, u32[]{:S(2)}) async-start(f32[1,64,512]{2,0,1:T(1,128)} %broadcast_in_dim_reshape_reshape.4), calls=%async_computation.2 | async-start | bytes 262144 | tf_op jit(solution)/shard_map/all_to_all | solution.py:231
  97.0 9.8 %copy-start.15 = (f32[512]{0:T(512)S(1)}, f32[512]{0:T(512)}, u32[]{:S(2)}) copy-start(f32[512]{0:T(512)} %mul.237) | copy-start | bytes 6148
  97.0 14.9 %copy-start.1 = (bf16[4,512,512]{2,1,0:T(8,128)(2,1)S(1)}, bf16[4,512,512]{2,1,0:T(8,128)(2,1)}, u32[]{:S(2)}) copy-start(bf16[4,512,512]{2,1,0:T(8,128)(2,1)} %param.31) | copy-start | bytes 6291460
  97.0 14.9 %copy-start.16 = (pred[4,512]{1,0:T(4,128)(4,1)S(1)}, pred[4,512]{1,0:T(4,128)(4,1)}, u32[]{:S(2)}) copy-start(pred[4,512]{1,0:T(4,128)(4,1)} %fusion.35) | copy-start | bytes 6148
  107.5 13.2 %all-to-all-start.5 = ((bf16[32,2,512]{2,1,0:T(2,128)(2,1)}), bf16[32,2,512]{2,1,0:T(2,128)(2,1)S(1)}, u32[]{:S(2)}, u32[]{:S(2)}) async-start(bf16[32,2,512]{2,1,0:T(2,128)(2,1)} %broadcast_in_dim.162), calls=%async_computation.5 | async-start | bytes 131072 | tf_op jit(solution)/shard_map/all_to_all | solution.py:19
  111.9 4.5 %copy-start.6 = (f32[64,8]{1,0:T(8,128)S(1)}, f32[64,8]{1,0:T(8,128)}, u32[]{:S(2)}) copy-start(f32[64,8]{1,0:T(8,128)} %copy-done.5) | copy-start | bytes 6148
where the time goes:
time: 132 us; the launch traced here: 131 us
  starting transfers between devices  36 us (27%)
  waiting for transfers between devices  34 us (26%)
  local copies, waits for them, and re-layouts  21.5 us (16%)
  other arithmetic  14.3 us (11%)
  matrix products  14.2 us (11%)
  blocking collectives  8.85 us (7%)
    all_to_all x2, waiting for transfers between devices, from_everyone(): lax.all_to_all(jnp.broadcast_to(array[None], (devices, *array.shape)), ax...  14.6 us
    all_to_all x1, starting transfers between devices, summed_on_arrival(): lax.all_to_all(parts, axis, split_axis=0, concat_axis=0, tiled=True)  11.9 us
    all_to_all x2, starting transfers between devices, from_everyone(): lax.all_to_all(jnp.broadcast_to(array[None], (devices, *array.shape)), ax...  10.1 us
    all_to_all x1, blocking collectives, from_everyone(): lax.all_to_all(jnp.broadcast_to(array[None], (devices, *array.shape)), ax...  8.85 us
    all_to_all x1, waiting for transfers between devices, shards(): lax.all_to_all(flat_max[None], 'kv', split_axis=1, concat_axis=0, tiled=T...  6.53 us
    unnamed x54, local copies, waits for them, and re-layouts  6.18 us
    all_to_all x1, starting transfers between devices, shards(): lax.all_to_all(flat_total[None], 'kv', split_axis=1, concat_axis=0, tiled...  5.57 us
    all_to_all x1, waiting for transfers between devices, shards(): lax.all_to_all(flat_total[None], 'kv', split_axis=1, concat_axis=0, tiled...  4.74 us
  transfers between devices with their start and end apart: 6, of which 6 were waited for; matrix products, arithmetic and copies ran while one was open for 22% of the time, Pallas kernels for 0%

commit v1 on v0

v1 whole, which is shorter than its diff:
```python
import functools

import jax
import jax.numpy as jnp
from jax import lax
from jax.experimental import pallas as pl
from jax.experimental.pallas import tpu as pltpu
from jax.sharding import PartitionSpec as P

EPSILON = 1e-06
MASKED = -1e30
MESH = pl.DeviceIdType.MESH
F32 = jnp.float32
BF16 = jnp.bfloat16

NZ, NX = 8, 4
N_KV = NZ * NX
SEQS, PROPS, HEADS, DH = 4, 16, 8, 64
ROWS = SEQS * PROPS
WIDTH = HEADS * DH
POS = 512
D = 2048
FEATS = D // N_KV
LANES = 128
FIRST_OWNER = 15341 // POS
CHUNK = 128
QN, GL, KVN, PS, NR, WO = 3, 7, 8, 9, 11, 15

OFFSETS = sorted(
    ((dz, dx) for dz in range(NZ) for dx in range(NX) if (dz, dx) != (0, 0)),
    key=lambda o: -(min(o[0], NZ - o[0]) + min(o[1], NX - o[1])),
)


def iota(shape, dim):
    return lax.broadcasted_iota(jnp.int32, shape, dim)


def swap(x):
    return pltpu.roll(x, DH, 1)


def dot(a, b, dims, precision=None):
    return lax.dot_general(
        a, b, (dims, ((), ())), preferred_element_type=F32, precision=precision
    )


def layer_kernel(
    tokens,
    norm_gain,
    w_query,
    w_key,
    w_value,
    w_forget,
    forget_bias,
    query_gain,
    key_gain,
    head_gain,
    w_out,
    key_cache,
    value_cache,
    gate_cache,
    lengths,
    accepted,
    parents,
    out_ref,
    gates_ref,
    kvn_ref,
    tok_v,
    w_v,
    wf_v,
    wo_v,
    ng_v,
    qg_v,
    kg_v,
    hg_v,
    par_v,
    fb_s,
    len_s,
    acc_s,
    k_v,
    v_v,
    g_v,
    q_send,
    q_recv,
    st_send,
    st_recv,
    kv_send,
    kv_recv,
    qn_send,
    qn_recv,
    kvn_send,
    kvn_recv,
    gl_send,
    gl_recv,
    p_send,
    p_recv,
    ps_send,
    ps_recv,
    n_send,
    n_recv,
    load_sem,
    ssem,
    rsem,
):
    me = lax.axis_index("kv")
    tp = lax.axis_index("tp")
    mz, mx = me // NX, me % NX
    peers = [((mz + dz) % NZ) * NX + (mx + dx) % NX for dz, dx in OFFSETS]
    s_me, h_me = me // HEADS, me % HEADS

    loads = []

    def load(src, dst):
        copy = pltpu.make_async_copy(src, dst, load_sem.at[len(loads)])
        copy.start()
        loads.append(copy)
        return copy

    first = [
        load(tokens, tok_v),
        load(norm_gain, ng_v),
        load(w_query, w_v.at[:, pl.ds(0, WIDTH)]),
        load(w_forget.at[:, pl.ds(pl.multiple_of(me // 2 * LANES, LANES), LANES)], wf_v),
        load(w_key, w_v.at[:, pl.ds(WIDTH, WIDTH)]),
        load(w_value, w_v.at[:, pl.ds(2 * WIDTH, WIDTH)]),
    ]
    barrier = pltpu.get_barrier_semaphore()
    for p in peers:
        for core in range(2):
            pl.semaphore_signal(
                barrier, inc=1, device_id={"kv": p, "tp": core}, device_id_type=MESH
            )
    pl.semaphore_signal(barrier, inc=1, device_id={"tp": 1 - tp}, device_id_type=MESH)
    small = [
        load(parents, par_v),
        load(forget_bias, fb_s),
        load(query_gain, qg_v),
        load(key_gain, kg_v),
        load(head_gain, hg_v),
        load(lengths, len_s),
        load(accepted, acc_s),
    ]
    out_load = load(w_out, wo_v.at[tp])
    cached = [load(key_cache, k_v), load(value_cache, v_v), load(gate_cache, g_v)]

    def send(src, dst, phase, kv, core=None, recv=None):
        pltpu.make_async_remote_copy(
            src_ref=src,
            dst_ref=dst,
            send_sem=ssem.at[phase],
            recv_sem=rsem.at[phase if recv is None else recv],
            device_id={"kv": kv} if core is None else {"kv": kv, "tp": core},
            device_id_type=MESH,
        ).start()

    def await_recv(buf, phase, count):
        part = buf.at[pl.ds(0, count)]
        pltpu.make_async_remote_copy(
            src_ref=part,
            dst_ref=part,
            send_sem=ssem.at[phase],
            recv_sem=rsem.at[phase],
            device_id={"kv": peers[0]},
            device_id_type=MESH,
        ).wait_recv()

    def await_send(buf, phase, count):
        part = buf.at[pl.ds(0, count)]
        pltpu.make_async_remote_copy(
            src_ref=part,
            dst_ref=part,
            send_sem=ssem.at[phase],
            recv_sem=rsem.at[phase],
            device_id={"kv": peers[0]},
            device_id_type=MESH,
        ).wait_send()

    low8 = iota((8, LANES), 1) < DH
    low16 = iota((16, LANES), 1) < DH

    for copy in first:
        copy.wait()
    rows = tok_v[...].reshape(ROWS, FEATS).astype(F32)
    scaled = (rows * ng_v[...].reshape(1, FEATS)).astype(BF16)
    summed = dot(scaled, w_v[...], ((1,), (0,)))
    forget = wf_v[...].astype(F32)
    forget = jnp.where(me % 2 == 1, swap(forget), forget)[:, :FEATS].astype(BF16)
    gate_part = dot(forget, scaled, ((1,), (1,)))
    squares = dot(
        jnp.ones((2 * HEADS, FEATS), F32), rows * rows, ((1,), (1,)), lax.Precision.HIGHEST
    )
    st_send[...] = jnp.concatenate([gate_part, squares], axis=1).reshape(2 * HEADS, 1, LANES)
    for s in range(SEQS):
        for t in range(HEADS // 2):
            a = summed[s * 16 : s * 16 + 8, t * LANES : (t + 1) * LANES]
            b = summed[s * 16 + 8 : s * 16 + 16, t * LANES : (t + 1) * LANES]
            q_send[s * HEADS + 2 * t] = jnp.where(low8, a, swap(b))
            q_send[s * HEADS + 2 * t + 1] = jnp.where(low8, swap(a), b)
    for s in range(SEQS):
        for t in range(HEADS // 2):
            at = WIDTH + t * LANES
            k = summed[s * 16 : s * 16 + 16, at : at + LANES]
            v = summed[s * 16 : s * 16 + 16, at + WIDTH : at + WIDTH + LANES]
            kv_send[s * HEADS + 2 * t] = jnp.where(low16, k, swap(v)).astype(BF16)
            kv_send[s * HEADS + 2 * t + 1] = jnp.where(low16, swap(k), v).astype(BF16)

    pl.semaphore_wait(barrier, 2 * N_KV - 1)

    for p in peers:
        send(q_send.at[p], q_recv.at[me], 0, p)
        send(st_send.at[tp * HEADS + p % HEADS], st_recv.at[me], 1, p)
    for p in peers:
        send(kv_send.at[p], kv_recv.at[me], 2, p)
    q_recv[me] = q_send[me]
    st_recv[me] = st_send[tp * HEADS + h_me]
    kv_recv[me] = kv_send[me]

    for copy in small:
        copy.wait()
    out_load.wait()
    send(wo_v.at[tp], wo_v.at[tp], WO, me, 1 - tp)

    parent_row = par_v[pl.ds(s_me, 1), :]
    step_t = (iota((PROPS, PROPS), 0) == parent_row).astype(BF16)
    eye = (iota((PROPS, PROPS), 0) == iota((PROPS, PROPS), 1)).astype(F32)
    ancestors_t = eye + step_t.astype(F32)
    power = step_t
    for _ in range(3):
        power = dot(power, power, ((1,), (0,))).astype(BF16)
        ancestors_t = ancestors_t + dot(ancestors_t.astype(BF16), power, ((1,), (0,)))
    ancestors = ancestors_t.T

    await_recv(st_recv, 1, N_KV - 1)
    stats = jnp.sum(st_recv[...].reshape(N_KV, LANES), axis=0, keepdims=True)
    inverse_row = lax.rsqrt(stats / D + EPSILON)
    logits = stats * swap(inverse_row) + fb_s[tp * HEADS + h_me]
    log_row = jnp.minimum(logits, 0.0) - jnp.log1p(jnp.exp(-jnp.abs(logits)))
    spot = s_me * PROPS
    at_row = iota((PROPS, LANES), 0) + spot
    at_lane = iota((PROPS, LANES), 1)
    inverse = jnp.sum(
        jnp.where(at_lane == at_row + ROWS, inverse_row, 0.0), axis=1, keepdims=True
    )
    own_log = jnp.sum(jnp.where(at_lane == at_row, log_row, 0.0), axis=1, keepdims=True)
    path_row = jnp.sum(ancestors_t * own_log, axis=0, keepdims=True)
    gl_send[...] = log_row

    await_recv(q_recv, 0, N_KV - 1)
    raw = jnp.sum(q_recv[...], axis=0) * jnp.where(low8, inverse[:8], inverse[8:])
    gain = qg_v[...].reshape(1, DH)
    gain = jnp.concatenate([gain, gain], axis=1)
    square = raw * raw
    mean_low = jnp.sum(jnp.where(low8, square, 0.0), axis=1, keepdims=True) / DH
    mean_high = jnp.sum(jnp.where(low8, 0.0, square), axis=1, keepdims=True) / DH
    q_packed = (raw * lax.rsqrt(jnp.where(low8, mean_low, mean_high) + EPSILON) * gain).astype(
        BF16
    )
    qn_send[...] = q_packed

    for p in peers:
        send(qn_send, qn_recv.at[me], QN, p, recv=QN + s_me)
    qn_recv[me] = q_packed

    @pl.when(s_me == 0)
    def _():
        for p in peers:
            send(gl_send, gl_recv.at[h_me], GL, p)
        gl_recv[h_me] = log_row

    await_recv(kv_recv, 2, N_KV - 1)
    raw_kv = jnp.sum(kv_recv[...].astype(F32), axis=0) * inverse
    mean_key = jnp.sum(jnp.where(low16, raw_kv * raw_kv, 0.0), axis=1, keepdims=True) / DH
    gain = kg_v[...].reshape(1, DH)
    gain = jnp.concatenate([gain, gain], axis=1)
    kv_new = jnp.where(low16, raw_kv * lax.rsqrt(mean_key + EPSILON) * gain, raw_kv).astype(BF16)
    kvn_send[...] = kv_new
    for owner in range(FIRST_OWNER, N_KV):

        @pl.when(me != owner)
        def _():
            send(kvn_send, kvn_recv.at[me], KVN, owner)

        @pl.when(me == owner)
        def _():
            kvn_recv[me] = kv_new

    q32 = q_packed.astype(F32)
    q_rows = jnp.concatenate(
        [jnp.where(low8, q32, 0.0), jnp.where(low8, swap(q32), 0.0)], axis=0
    ).astype(BF16)
    tree = dot(q_rows, kv_new, ((1,), (1,))) * DH**-0.5 - path_row
    tree_live = ancestors > 0.5
    tree = jnp.where(tree_live, tree, MASKED)
    tree_max = jnp.max(tree, axis=1, keepdims=True)
    tree_weights = jnp.where(tree_live, jnp.exp(tree - tree_max), 0.0)
    tree_total = jnp.sum(tree_weights, axis=1, keepdims=True)
    tree_sum = dot(tree_weights.astype(BF16), kv_new, ((1,), (0,)))
    tree_packed = jnp.where(low8, swap(tree_sum[:8]), tree_sum[8:])

    for copy in cached:
        copy.wait()
    pos = iota((1, POS), 1) + me * POS
    diag = iota((PROPS, LANES), 1) - iota((PROPS, LANES), 0)
    corner = (iota((PROPS, LANES), 0) == 0) & (iota((PROPS, LANES), 1) == 2 * PROPS)
    for turn in (0, 1, 3, 2):
        s = (s_me + turn) % SEQS
        await_recv(qn_recv, QN + s, HEADS if turn else HEADS - 1)
        base = len_s[s] + acc_s[s]
        live = pos < base
        gates = g_v[s]
        bound = jnp.sum(jnp.where(pos == base - 1, gates, 0.0), axis=1, keepdims=True)
        for t in range(HEADS // 2):
            m0 = qn_recv[s * HEADS + 2 * t].astype(F32)
            m1 = qn_recv[s * HEADS + 2 * t + 1].astype(F32)
            lhs = jnp.concatenate(
                [
                    jnp.where(low8, m0, 0.0),
                    jnp.where(low8, swap(m0), 0.0),
                    jnp.where(low8, 0.0, swap(m1)),
                    jnp.where(low8, 0.0, m1),
                ],
                axis=0,
            ).astype(BF16)
            keys = k_v[s, :, pl.ds(t * LANES, LANES)]
            values = v_v[s, :, pl.ds(t * LANES, LANES)]
            scores = dot(lhs, keys, ((1,), (1,))) * DH**-0.5
            gate_rows = jnp.concatenate(
                [
                    jnp.broadcast_to(gates[2 * t : 2 * t + 1], (PROPS, POS)),
                    jnp.broadcast_to(gates[2 * t + 1 : 2 * t + 2], (PROPS, POS)),
                ],
                axis=0,
            )
            scores = jnp.where(live, scores - gate_rows, MASKED)
            peak = jnp.max(scores, axis=1, keepdims=True)
            weights = jnp.where(live, jnp.exp(scores - peak), 0.0)
            total = jnp.sum(weights, axis=1, keepdims=True)
            part = dot(weights.astype(BF16), values, ((1,), (0,)))
            p_send[s * HEADS + 2 * t] = jnp.where(low8, part[:8], swap(part[8:16]))
            p_send[s * HEADS + 2 * t + 1] = jnp.where(low8, swap(part[16:24]), part[24:32])
            for odd in range(2):
                rows_at = slice(odd * PROPS, (odd + 1) * PROPS)
                head = 2 * t + odd
                tile = jnp.where(diag == 0, peak[rows_at], 0.0)
                tile = jnp.where(diag == PROPS, total[rows_at], tile)
                tile = jnp.where(corner, bound[head : head + 1], tile)
                ps_send[s * HEADS + head] = jnp.sum(tile, axis=0, keepdims=True)
        for j in range(HEADS):
            if turn == 0 and j == 0:
                continue
            target = s * HEADS + (h_me + j) % HEADS
            send(p_send.at[target], p_recv.at[me], PS, target)
            send(ps_send.at[target], ps_recv.at[me], PS + 1, target)
    p_recv[me] = p_send[me]
    ps_recv[me] = ps_send[me]

    await_recv(ps_recv, PS + 1, N_KV - 1)
    stats_t = ps_recv[...].reshape(N_KV, LANES).T
    peaks = stats_t[:PROPS]
    bound = jnp.sum(stats_t[2 * PROPS : 2 * PROPS + 1], axis=1, keepdims=True)
    tree_max = tree_max - bound
    top = jnp.maximum(jnp.max(peaks, axis=1, keepdims=True), tree_max)
    factors = jnp.exp(peaks - top)
    tree_factor = jnp.exp(tree_max - top)
    total = (
        jnp.sum(factors * stats_t[PROPS : 2 * PROPS], axis=1, keepdims=True)
        + tree_total * tree_factor
    )
    await_recv(p_recv, PS, N_KV - 1)
    acc = [tree_packed * jnp.where(low8, tree_factor[:8], tree_factor[8:])] + [None] * 3
    for i in range(N_KV):
        factor = jnp.where(low8, factors[:8, i : i + 1], factors[8:, i : i + 1])
        term = p_recv[i] * factor
        acc[i % 4] = term if acc[i % 4] is None else acc[i % 4] + term
    weighted = (acc[0] + acc[1]) + (acc[2] + acc[3])
    attended = weighted / jnp.where(low8, total[:8], total[8:])
    square = attended * attended
    mean_low = jnp.sum(jnp.where(low8, square, 0.0), axis=1, keepdims=True) / DH
    mean_high = jnp.sum(jnp.where(low8, 0.0, square), axis=1, keepdims=True) / DH
    gain = hg_v[...].reshape(1, DH)
    gain = jnp.concatenate([gain, gain], axis=1)
    normed = (
        attended * lax.rsqrt(jnp.where(low8, mean_low, mean_high) + EPSILON) * gain
    ).astype(BF16)
    n_send[...] = normed

    slot = tp * N_KV + me
    for p in peers:
        for core in range(2):
            send(n_send, n_recv.at[slot], NR, p, core, recv=NR + s_me)
    send(n_send, n_recv.at[slot], NR, me, 1 - tp, recv=NR + s_me)
    n_recv[slot] = normed

    @pl.when(s_me == 0)
    def _():
        await_recv(gl_recv, GL, HEADS - 1)

    @pl.when(s_me != 0)
    def _():
        await_recv(gl_recv, GL, HEADS)

    logs = gl_recv[...].reshape(HEADS, LANES)
    for s in range(SEQS):
        gates_ref[s] = logs[:, s * PROPS : (s + 1) * PROPS]

    @pl.when(me >= FIRST_OWNER)
    def _():
        await_recv(kvn_recv, KVN, N_KV - 1)
        kvn_ref[...] = kvn_recv[...]

    @pl.when(me < FIRST_OWNER)
    def _():
        kvn_ref[...] = jnp.zeros_like(kvn_ref)

    await_recv(wo_v, WO, 1)
    for turn in (0, 1, 3, 2):
        s = (s_me + turn) % SEQS
        await_recv(n_recv, NR + s, 2 * HEADS if turn else 2 * HEADS - 1)
        layer_sum = None
        for core in range(2):
            tiles = []
            for t in range(HEADS // 2):
                m0 = n_recv[core * N_KV + s * HEADS + 2 * t].astype(F32)
                m1 = n_recv[core * N_KV + s * HEADS + 2 * t + 1].astype(F32)
                tiles.append(
                    jnp.concatenate(
                        [jnp.where(low8, m0, swap(m1)), jnp.where(low8, swap(m0), m1)], axis=0
                    ).astype(BF16)
                )
            term = dot(jnp.concatenate(tiles, axis=1), wo_v[core], ((1,), (1,)))
            term = term.astype(BF16).astype(F32)
            layer_sum = term if layer_sum is None else layer_sum + term
        out_ref[s] = layer_sum.astype(BF16)

    await_send(q_send, 0, N_KV - 1)
    await_send(st_recv, 1, N_KV - 1)
    await_send(kv_send, 2, N_KV - 1)
    await_send(qn_recv, QN, N_KV - 1)
    await_send(wo_v, WO, 1)

    @pl.when(s_me == 0)
    def _():
        await_send(st_recv, GL, N_KV - 1)

    @pl.when(me >= FIRST_OWNER)
    def _():
        await_send(kvn_recv, KVN, N_KV - FIRST_OWNER - 1)

    @pl.when(me < FIRST_OWNER)
    def _():
        await_send(kvn_recv, KVN, N_KV - FIRST_OWNER)

    await_send(p_send, PS, N_KV - 1)
    await_send(ps_send, PS + 1, N_KV - 1)
    await_send(n_recv, NR, 2 * N_KV - 1)


def cache_kernel(
    key_cache,
    value_cache,
    kvn,
    lengths,
    accepted,
    layer_in,
    gates_in,
    layer_out,
    new_keys,
    new_values,
    gates_out,
    k_v,
    v_v,
    sem,
):
    me = lax.axis_index("kv")
    sides = ((key_cache, k_v, new_keys), (value_cache, v_v, new_values))
    ends = [
        pltpu.make_async_copy(layer_in, layer_out, sem.at[0]),
        pltpu.make_async_copy(gates_in, gates_out, sem.at[1]),
    ]

    def write(s, c, side, patched):
        src, buf, dst = sides[side]
        rows = pl.ds(pl.multiple_of(c * CHUNK, CHUNK), CHUNK)
        return pltpu.make_async_copy(
            (buf if patched else src).at[s, rows], dst.at[s, rows], sem.at[2 + s]
        )

    for s in range(SEQS):
        offset = lengths[s] + accepted[s] - me * POS
        for c in range(POS // CHUNK):
            clear = (offset >= (c + 1) * CHUNK) | (offset + PROPS <= c * CHUNK)

            @pl.when(clear)
            def _():
                for side in range(2):
                    write(s, c, side, False).start()

    for copy in ends:
        copy.start()
    low = iota((CHUNK, LANES), 1) < DH

    @pl.when(me >= FIRST_OWNER)
    def _():
        for s in range(SEQS):
            offset = lengths[s] + accepted[s] - me * POS

            def patch(c):
                slot = iota((CHUNK, 1), 0) + c * CHUNK - offset
                hit = (slot >= 0) & (slot < PROPS)
                placing = (slot == iota((CHUNK, PROPS), 1)).astype(BF16)
                rows = pl.ds(pl.multiple_of(c * CHUNK, CHUNK), CHUNK)
                for t in range(HEADS // 2):
                    w0 = dot(placing, kvn[s * HEADS + 2 * t], ((1,), (0,)))
                    w1 = dot(placing, kvn[s * HEADS + 2 * t + 1], ((1,), (0,)))
                    at = (s, rows, pl.ds(t * LANES, LANES))
                    k_v[at] = jnp.where(
                        hit, jnp.where(low, w0, swap(w1)), key_cache[at].astype(F32)
                    ).astype(BF16)
                    v_v[at] = jnp.where(
                        hit, jnp.where(low, swap(w0), w1), value_cache[at].astype(F32)
                    ).astype(BF16)
                for side in range(2):
                    write(s, c, side, True).start()

            first = jnp.maximum(offset, 0) // CHUNK
            last = jnp.minimum(offset + PROPS - 1, POS - 1) // CHUNK

            @pl.when((offset > -PROPS) & (offset < POS))
            def _():
                patch(first)

                @pl.when(last > first)
                def _():
                    patch(last)

    for s in range(SEQS):
        for src, _, dst in sides:
            pltpu.make_async_copy(src.at[s], dst.at[s], sem.at[2 + s]).wait()
    for copy in ends:
        copy.wait()


def shards(*args):
    hbm = pl.BlockSpec(memory_space=pltpu.HBM)
    vmem = pl.BlockSpec(memory_space=pltpu.VMEM)
    smem = pl.BlockSpec(memory_space=pltpu.SMEM)
    operands = list(args)
    operands[5] = operands[5].T
    operands[10] = operands[10].T
    operands = [pltpu.with_memory_space_constraint(a, pltpu.HBM) for a in operands]
    layer_out, gates, kvn = pl.pallas_call(
        layer_kernel,
        out_shape=(
            jax.ShapeDtypeStruct((SEQS, PROPS, FEATS), BF16),
            jax.ShapeDtypeStruct((SEQS, HEADS, PROPS), F32),
            jax.ShapeDtypeStruct((N_KV, PROPS, LANES), BF16),
        ),
        in_specs=[hbm] * len(operands),
        out_specs=(vmem, vmem, vmem),
        scratch_shapes=[
            pltpu.VMEM((SEQS, PROPS, FEATS), BF16),
            pltpu.VMEM((FEATS, 3 * WIDTH), BF16),
            pltpu.VMEM((2 * HEADS, LANES), BF16),
            pltpu.VMEM((2, FEATS, WIDTH), BF16),
            pltpu.VMEM((FEATS,), F32),
            pltpu.VMEM((DH,), F32),
            pltpu.VMEM((DH,), F32),
            pltpu.VMEM((DH,), F32),
            pltpu.VMEM((SEQS, PROPS), jnp.int32),
            pltpu.SMEM((2 * HEADS,), F32),
            pltpu.SMEM((SEQS,), jnp.int32),
            pltpu.SMEM((SEQS,), jnp.int32),
            pltpu.VMEM((SEQS, POS, WIDTH), BF16),
            pltpu.VMEM((SEQS, POS, WIDTH), BF16),
            pltpu.VMEM((SEQS, HEADS, POS), F32),
            pltpu.VMEM((N_KV, 8, LANES), F32),
            pltpu.VMEM((N_KV, 8, LANES), F32),
            pltpu.VMEM((2 * HEADS, 1, LANES), F32),
            pltpu.VMEM((N_KV, 1, LANES), F32),
            pltpu.VMEM((N_KV, PROPS, LANES), BF16),
            pltpu.VMEM((N_KV, PROPS, LANES), BF16),
            pltpu.VMEM((8, LANES), BF16),
            pltpu.VMEM((N_KV, 8, LANES), BF16),
            pltpu.VMEM((PROPS, LANES), BF16),
            pltpu.VMEM((N_KV, PROPS, LANES), BF16),
            pltpu.VMEM((1, LANES), F32),
            pltpu.VMEM((HEADS, 1, LANES), F32),
            pltpu.VMEM((N_KV, 8, LANES), F32),
            pltpu.VMEM((N_KV, 8, LANES), F32),
            pltpu.VMEM((N_KV, 1, LANES), F32),
            pltpu.VMEM((N_KV, 1, LANES), F32),
            pltpu.VMEM((8, LANES), BF16),
            pltpu.VMEM((2 * N_KV, 8, LANES), BF16),
            pltpu.SemaphoreType.DMA((20,)),
            pltpu.SemaphoreType.DMA((24,)),
            pltpu.SemaphoreType.DMA((24,)),
        ],
        compiler_params=pltpu.CompilerParams(
            collective_id=0, has_side_effects=True, vmem_limit_bytes=24 * 2**20
        ),
        name="layer",
    )(*operands)
    key_cache, value_cache, lengths, accepted = args[11], args[12], args[14], args[15]
    layer_out, new_keys, new_values, gates = pl.pallas_call(
        cache_kernel,
        out_shape=(
            jax.ShapeDtypeStruct(layer_out.shape, BF16),
            jax.ShapeDtypeStruct(key_cache.shape, BF16),
            jax.ShapeDtypeStruct(value_cache.shape, BF16),
            jax.ShapeDtypeStruct(gates.shape, F32),
        ),
        in_specs=[vmem, vmem, vmem, smem, smem, vmem, vmem],
        out_specs=(hbm, hbm, hbm, hbm),
        scratch_shapes=[
            pltpu.VMEM((SEQS, POS, WIDTH), BF16),
            pltpu.VMEM((SEQS, POS, WIDTH), BF16),
            pltpu.SemaphoreType.DMA((2 + SEQS,)),
        ],
        compiler_params=pltpu.CompilerParams(vmem_limit_bytes=16 * 2**20),
        name="cache",
    )(key_cache, value_cache, kvn, lengths, accepted, layer_out, gates)
    return layer_out, new_keys, new_values, jnp.transpose(gates, (0, 2, 1))


def solution(mesh):
    placed = (
        P("dp", None, "kv"),
        P("kv"),
        P("kv", "tp"),
        P("kv", "tp"),
        P("kv", "tp"),
        P(),
        P(),
        P(),
        P(),
        P(),
        P("tp", "kv"),
        P("dp", "kv", "tp"),
        P("dp", "kv", "tp"),
        P("dp", "tp", "kv"),
        P("dp"),
        P("dp"),
        P("dp", None),
    )
    return jax.shard_map(
        shards,
        mesh=mesh,
        in_specs=placed,
        out_specs=(
            P("dp", None, "kv"),
            P("dp", "kv", "tp"),
            P("dp", "kv", "tp"),
            P("dp", None, "tp"),
        ),
        check_vma=False,
    )
```

time: 132 us -> 44.8 us (0.34)
  Pallas kernels: 0 us -> 44 us
  starting transfers between devices: 36 us -> 0 us
  waiting for transfers between devices: 34 us -> 0 us
  local copies, waits for them, and re-layouts: 21.5 us -> 0.02 us
  other arithmetic: 14.3 us -> 0 us
  matrix products: 14.2 us -> 0 us
  blocking collectives: 8.85 us -> 0 us
    pallas_call x0 -> x2, Pallas kernels: none -> 44 us  [the longest x1 41.4 us: shards(): pl.pallas_call(layer_kernel, out_shape=(jax.ShapeDtypeStruct((SEQS, PROPS...]
    all_to_all x6 -> x0, starting transfers between devices: 36 us -> none  [the longest x1 11.9 us: summed_on_arrival(): lax.all_to_all(parts, axis, split_axis=0, concat_axis=0, tiled=True)]
    all_to_all x6 -> x0, waiting for transfers between devices: 34 us -> none  [the longest x2 14.6 us: from_everyone(): lax.all_to_all(jnp.broadcast_to(array[None], (devices, *array.shape)), ax...]
    dot_general x25 -> x0, matrix products: 14.2 us -> none  [the longest x16 3.68 us: extend(): jnp.einsum('sij,sjk->sik', step_matrix, ancestors, precision=lax.Precisio...]
    all_to_all x1 -> x0, blocking collectives: 8.85 us -> none  [from_everyone(): lax.all_to_all(jnp.broadcast_to(array[None], (devices, *array.shape)), ax...]
    unnamed x54 -> x8, local copies, waits for them, and re-layouts: 6.18 us -> 0.02 us
    slice x3 -> x0, local copies, waits for them, and re-layouts: 4.48 us -> none  [the longest x2 3.54 us: packed_total(): total[b:e].reshape(a.shape)]
    select_n x1 -> x0, other arithmetic: 4.45 us -> none  [shards(): new_values = jnp.where(hit_rows, written[..., head_width:], value_cache)]
  transfers between devices with their start and end apart: 6 -> 0, of which waited for: 6 -> 0; matrix products, arithmetic and copies ran while one was open for 22% -> 0% of each run, Pallas kernels for 0% -> 0%
where the time goes in v1:
time: 44.8 us; the launch traced here: 44.7 us
  Pallas kernels  44 us (98%)
  between operations  0.71 us (2%)
    pallas_call x1, Pallas kernels, shards(): pl.pallas_call(layer_kernel, out_shape=(jax.ShapeDtypeStruct((SEQS, PROPS...  41.4 us
    pallas_call x1, Pallas kernels, shards(): pl.pallas_call(cache_kernel, out_shape=(jax.ShapeDtypeStruct(layer_out.sh...  2.59 us

profile of v1, /device:TPU:1, one launch (start us, length us, event | category | flops | bytes accessed | tf_op | source)
XLA Modules:
  0.0 44.7 jit_solution(14763511556291035055)
XLA Ops:
  0.6 0.0 copy-start
  0.6 0.0 copy-start.1
  0.7 0.0 copy-start.2
  0.7 0.0 copy-start.3
  0.7 41.4 %layer.1 = (bf16[4,16,64]{2,1,0:T(8,128)(2,1)S(1)}, f32[4,8,16]{2,1,0:T(8,128)S(1)}, bf16[32,16,128]{2,1,0:T(8,128)(2,1)S(1)}) custom-call(bf16[4,16,64]{2,1,0:T(8,128)(2,1)} %tokens.1, f32[64]{0:T(128)} %norm_gain.1, bf16[64,512]{1,0:T(8,128)(2,1)} %w_query.1, bf16[64,512]{1,0:T(8,128)(2,1)} %w_key.1, bf16[64,512]{1,0:T(8,128)(2,1)} %w_value.1, ...), custom_call_target="tpu_custom_call" | custom-call | tf_op jit(solution)/shard_map/layer/pallas_call | solution.py:553
  42.1 0.0 copy-done
  42.1 0.0 copy-done.1
  42.1 0.0 copy-done.2
  42.1 0.0 copy-done.3
  42.1 2.6 %cache.1 = (bf16[4,16,64]{2,1,0:T(8,128)(2,1)}, bf16[4,512,512]{2,1,0:T(8,128)(2,1)}, bf16[4,512,512]{2,1,0:T(8,128)(2,1)}, f32[4,8,16]{2,1,0:T(8,128)}) custom-call(bf16[4,512,512]{2,1,0:T(8,128)(2,1)S(1)} %copy-done, bf16[4,512,512]{2,1,0:T(8,128)(2,1)S(1)} %copy-done.1, bf16[32,16,128]{2,1,0:T(8,128)(2,1)S(1)} %get-tuple-element.11.kvn, s32[4]{0:T(128)S(1)} %copy-done.2, ...), custom_call_target="tpu_custom_call" | custom-call | tf_op jit(solution)/shard_map/cache/pallas_call | solution.py:606
Async XLA Ops:
  0.6 41.4 %copy-start = (bf16[4,512,512]{2,1,0:T(8,128)(2,1)S(1)}, bf16[4,512,512]{2,1,0:T(8,128)(2,1)}, u32[]{:S(2)}) copy-start(bf16[4,512,512]{2,1,0:T(8,128)(2,1)} %key_cache.3) | copy-start | bytes 6291460
  0.6 41.4 %copy-start.1 = (bf16[4,512,512]{2,1,0:T(8,128)(2,1)S(1)}, bf16[4,512,512]{2,1,0:T(8,128)(2,1)}, u32[]{:S(2)}) copy-start(bf16[4,512,512]{2,1,0:T(8,128)(2,1)} %value_cache.3) | copy-start | bytes 6291460
  0.7 41.4 %copy-start.2 = (s32[4]{0:T(128)S(1)}, s32[4]{0:T(128)}, u32[]{:S(2)}) copy-start(s32[4]{0:T(128)} %lengths.3) | copy-start | bytes 52
  0.7 41.4 %copy-start.3 = (s32[4]{0:T(128)S(1)}, s32[4]{0:T(128)}, u32[]{:S(2)}) copy-start(s32[4]{0:T(128)} %accepted.3) | copy-start | bytes 52

commit v2 on v1

--- a/solution.py
+++ b/solution.py
@@ -24,12 +24,17 @@
 LANES = 128
 FIRST_OWNER = 15341 // POS
 CHUNK = 128
-QN, GL, KVN, PS, NR, WO = 3, 7, 8, 9, 11, 15
+QN, GL, KVN, PS, NR, WO, KVZ, TR = 3, 7, 8, 9, 11, 13, 14, 15
 
 OFFSETS = sorted(
     ((dz, dx) for dz in range(NZ) for dx in range(NX) if (dz, dx) != (0, 0)),
     key=lambda o: -(min(o[0], NZ - o[0]) + min(o[1], NX - o[1])),
 )
+
+
+NEAR = [o for o in [(0, 0)] + OFFSETS[::-1] if o[0] in (NZ - 2, NZ - 1, 0, 1)][::-1]
+AROUND = [(dz, dx) for dz in (NZ - 2, NZ - 1, 0, 1, 2) for dx in range(NX)]
+HALF = N_KV // 2
 
 
 def iota(shape, dim):
@@ -87,7 +92,9 @@
     st_send,
     st_recv,
     kv_send,
-    kv_recv,
+    kvx_recv,
+    kvz_send,
+    kvz_recv,
     qn_send,
     qn_recv,
     kvn_send,
@@ -98,6 +105,8 @@
     p_recv,
     ps_send,
     ps_recv,
+    t_buf,
+    ts_buf,
     n_send,
     n_recv,
     load_sem,
@@ -107,8 +116,13 @@
     me = lax.axis_index("kv")
     tp = lax.axis_index("tp")
     mz, mx = me // NX, me % NX
-    peers = [((mz + dz) % NZ) * NX + (mx + dx) % NX for dz, dx in OFFSETS]
+
+    def at(offset):
+        return ((mz + offset[0]) % NZ) * NX + (mx + offset[1]) % NX
+
+    peers = [at(o) for o in OFFSETS]
     s_me, h_me = me // HEADS, me % HEADS
+    pair, half = me % HALF, me // HALF
 
     loads = []
 
@@ -128,11 +142,11 @@
     ]
     barrier = pltpu.get_barrier_semaphore()
     for p in peers:
-        for core in range(2):
-            pl.semaphore_signal(
-                barrier, inc=1, device_id={"kv": p, "tp": core}, device_id_type=MESH
-            )
-    pl.semaphore_signal(barrier, inc=1, device_id={"tp": 1 - tp}, device_id_type=MESH)
+        pl.semaphore_signal(barrier, inc=1, device_id={"kv": p}, device_id_type=MESH)
+    for o in AROUND:
+        pl.semaphore_signal(
+            barrier, inc=1, device_id={"kv": at(o), "tp": 1 - tp}, device_id_type=MESH
+        )
     small = [
         load(parents, par_v),
         load(forget_bias, fb_s),
@@ -200,22 +214,25 @@
             q_send[s * HEADS + 2 * t + 1] = jnp.where(low8, swap(a), b)
     for s in range(SEQS):
         for t in range(HEADS // 2):
-            at = WIDTH + t * LANES
-            k = summed[s * 16 : s * 16 + 16, at : at + LANES]
-            v = summed[s * 16 : s * 16 + 16, at + WIDTH : at + WIDTH + LANES]
-            kv_send[s * HEADS + 2 * t] = jnp.where(low16, k, swap(v)).astype(BF16)
-            kv_send[s * HEADS + 2 * t + 1] = jnp.where(low16, swap(k), v).astype(BF16)
-
-    pl.semaphore_wait(barrier, 2 * N_KV - 1)
+            col = WIDTH + t * LANES
+            k = summed[s * 16 : s * 16 + 16, col : col + LANES]
+            v = summed[s * 16 : s * 16 + 16, col + WIDTH : col + WIDTH + LANES]
+            for head, tile in (
+                (2 * t, jnp.where(low16, k, swap(v))),
+                (2 * t + 1, jnp.where(low16, swap(k), v)),
+            ):
+                kv_send[head % NX, s * HEADS // NX + head // NX] = tile
+
+    pl.semaphore_wait(barrier, len(OFFSETS) + len(AROUND))
 
     for p in peers:
         send(q_send.at[p], q_recv.at[me], 0, p)
         send(st_send.at[tp * HEADS + p % HEADS], st_recv.at[me], 1, p)
-    for p in peers:
-        send(kv_send.at[p], kv_recv.at[me], 2, p)
+    for dx in (2, 1, 3):
+        other = (mx + dx) % NX
+        send(kv_send.at[other], kvx_recv.at[mx], 2, at((0, dx)))
     q_recv[me] = q_send[me]
     st_recv[me] = st_send[tp * HEADS + h_me]
-    kv_recv[me] = kv_send[me]
 
     for copy in small:
         copy.wait()
@@ -269,35 +286,13 @@
             send(gl_send, gl_recv.at[h_me], GL, p)
         gl_recv[h_me] = log_row
 
-    await_recv(kv_recv, 2, N_KV - 1)
-    raw_kv = jnp.sum(kv_recv[...].astype(F32), axis=0) * inverse
-    mean_key = jnp.sum(jnp.where(low16, raw_kv * raw_kv, 0.0), axis=1, keepdims=True) / DH
-    gain = kg_v[...].reshape(1, DH)
-    gain = jnp.concatenate([gain, gain], axis=1)
-    kv_new = jnp.where(low16, raw_kv * lax.rsqrt(mean_key + EPSILON) * gain, raw_kv).astype(BF16)
-    kvn_send[...] = kv_new
-    for owner in range(FIRST_OWNER, N_KV):
-
-        @pl.when(me != owner)
-        def _():
-            send(kvn_send, kvn_recv.at[me], KVN, owner)
-
-        @pl.when(me == owner)
-        def _():
-            kvn_recv[me] = kv_new
-
-    q32 = q_packed.astype(F32)
-    q_rows = jnp.concatenate(
-        [jnp.where(low8, q32, 0.0), jnp.where(low8, swap(q32), 0.0)], axis=0
-    ).astype(BF16)
-    tree = dot(q_rows, kv_new, ((1,), (1,))) * DH**-0.5 - path_row
-    tree_live = ancestors > 0.5
-    tree = jnp.where(tree_live, tree, MASKED)
-    tree_max = jnp.max(tree, axis=1, keepdims=True)
-    tree_weights = jnp.where(tree_live, jnp.exp(tree - tree_max), 0.0)
-    tree_total = jnp.sum(tree_weights, axis=1, keepdims=True)
-    tree_sum = dot(tree_weights.astype(BF16), kv_new, ((1,), (0,)))
-    tree_packed = jnp.where(low8, swap(tree_sum[:8]), tree_sum[8:])
+    await_recv(kvx_recv, 2, NX - 1)
+    part = kv_send[mx]
+    for dx in (1, 2, 3):
+        part = part + kvx_recv[(mx + dx) % NX]
+    kvz_send[...] = part
+    for dz in (4, 3, 5, 2, 6, 1, 7):
+        send(kvz_send.at[(mz + dz) % NZ], kvz_recv.at[mz], KVZ, at((dz, 0)))
 
     for copy in cached:
         copy.wait()
@@ -338,60 +333,112 @@
             weights = jnp.where(live, jnp.exp(scores - peak), 0.0)
             total = jnp.sum(weights, axis=1, keepdims=True)
             part = dot(weights.astype(BF16), values, ((1,), (0,)))
-            p_send[s * HEADS + 2 * t] = jnp.where(low8, part[:8], swap(part[8:16]))
-            p_send[s * HEADS + 2 * t + 1] = jnp.where(low8, swap(part[16:24]), part[24:32])
+            at_pair = s % 2 * HEADS + 2 * t
+            p_send[at_pair, s // 2] = jnp.where(low8, part[:8], swap(part[8:16])).astype(BF16)
+            p_send[at_pair + 1, s // 2] = jnp.where(
+                low8, swap(part[16:24]), part[24:32]
+            ).astype(BF16)
             for odd in range(2):
                 rows_at = slice(odd * PROPS, (odd + 1) * PROPS)
                 head = 2 * t + odd
                 tile = jnp.where(diag == 0, peak[rows_at], 0.0)
                 tile = jnp.where(diag == PROPS, total[rows_at], tile)
                 tile = jnp.where(corner, bound[head : head + 1], tile)
-                ps_send[s * HEADS + head] = jnp.sum(tile, axis=0, keepdims=True)
-        for j in range(HEADS):
-            if turn == 0 and j == 0:
-                continue
-            target = s * HEADS + (h_me + j) % HEADS
-            send(p_send.at[target], p_recv.at[me], PS, target)
-            send(ps_send.at[target], ps_recv.at[me], PS + 1, target)
-    p_recv[me] = p_send[me]
-    ps_recv[me] = ps_send[me]
-
-    await_recv(ps_recv, PS + 1, N_KV - 1)
-    stats_t = ps_recv[...].reshape(N_KV, LANES).T
-    peaks = stats_t[:PROPS]
-    bound = jnp.sum(stats_t[2 * PROPS : 2 * PROPS + 1], axis=1, keepdims=True)
-    tree_max = tree_max - bound
-    top = jnp.maximum(jnp.max(peaks, axis=1, keepdims=True), tree_max)
-    factors = jnp.exp(peaks - top)
-    tree_factor = jnp.exp(tree_max - top)
-    total = (
-        jnp.sum(factors * stats_t[PROPS : 2 * PROPS], axis=1, keepdims=True)
-        + tree_total * tree_factor
-    )
-    await_recv(p_recv, PS, N_KV - 1)
-    acc = [tree_packed * jnp.where(low8, tree_factor[:8], tree_factor[8:])] + [None] * 3
-    for i in range(N_KV):
-        factor = jnp.where(low8, factors[:8, i : i + 1], factors[8:, i : i + 1])
-        term = p_recv[i] * factor
-        acc[i % 4] = term if acc[i % 4] is None else acc[i % 4] + term
-    weighted = (acc[0] + acc[1]) + (acc[2] + acc[3])
-    attended = weighted / jnp.where(low8, total[:8], total[8:])
-    square = attended * attended
-    mean_low = jnp.sum(jnp.where(low8, square, 0.0), axis=1, keepdims=True) / DH
-    mean_high = jnp.sum(jnp.where(low8, 0.0, square), axis=1, keepdims=True) / DH
+                ps_send[s % 2 * HEADS + head, s // 2] = jnp.sum(tile, axis=0, keepdims=True)
+        if turn not in (2, 3):
+            continue
+        for side in (s, (s + 2) % SEQS):
+            for j in range(HEADS):
+                if turn == 2 and side is not s and j == 0:
+                    continue
+                head = (h_me + j) % HEADS
+                target = side * HEADS + head
+                send(p_send.at[s % 2 * HEADS + head], p_recv.at[me], PS, target)
+                send(ps_send.at[s % 2 * HEADS + head], ps_recv.at[me], PS + 1, target)
+    p_recv[me] = p_send[pair]
+    ps_recv[me] = ps_send[pair]
+
+    await_recv(kvz_recv, KVZ, NZ - 1)
+    raw_kv = kvz_send[mz]
+    for dz in range(1, NZ):
+        raw_kv = raw_kv + kvz_recv[(mz + dz) % NZ]
+    raw_kv = raw_kv * inverse
+    mean_key = jnp.sum(jnp.where(low16, raw_kv * raw_kv, 0.0), axis=1, keepdims=True) / DH
+    gain = kg_v[...].reshape(1, DH)
+    gain = jnp.concatenate([gain, gain], axis=1)
+    kv_new = jnp.where(low16, raw_kv * lax.rsqrt(mean_key + EPSILON) * gain, raw_kv).astype(BF16)
+    kvn_send[...] = kv_new
+    for owner in range(FIRST_OWNER, N_KV):
+
+        @pl.when(me != owner)
+        def _():
+            send(kvn_send, kvn_recv.at[me], KVN, owner)
+
+        @pl.when(me == owner)
+        def _():
+            kvn_recv[me] = kv_new
+
+    q32 = q_packed.astype(F32)
+    q_rows = jnp.concatenate(
+        [jnp.where(low8, q32, 0.0), jnp.where(low8, swap(q32), 0.0)], axis=0
+    ).astype(BF16)
+    tree = dot(q_rows, kv_new, ((1,), (1,))) * DH**-0.5 - path_row
+    tree_live = ancestors > 0.5
+    tree = jnp.where(tree_live, tree, MASKED)
+    mirror = (me + HALF) % N_KV
+    tree_max = jnp.max(tree, axis=1, keepdims=True)
+    tree_weights = jnp.where(tree_live, jnp.exp(tree - tree_max), 0.0)
+    tree_total = jnp.sum(tree_weights, axis=1, keepdims=True)
+    tree_sum = dot(tree_weights.astype(BF16), kv_new, ((1,), (0,)))
+    tree_packed = jnp.where(low8, swap(tree_sum[:8]), tree_sum[8:])
+    t_buf[half] = tree_packed
+    tile = jnp.where(diag == 0, tree_max, 0.0)
+    tile = jnp.where(diag == PROPS, tree_total, tile)
+    ts_buf[half] = jnp.sum(tile, axis=0, keepdims=True)
+    send(t_buf.at[half], t_buf.at[half], TR, mirror)
+    send(ts_buf.at[half], ts_buf.at[half], TR + 1, mirror)
+
     gain = hg_v[...].reshape(1, DH)
     gain = jnp.concatenate([gain, gain], axis=1)
-    normed = (
-        attended * lax.rsqrt(jnp.where(low8, mean_low, mean_high) + EPSILON) * gain
-    ).astype(BF16)
-    n_send[...] = normed
-
-    slot = tp * N_KV + me
-    for p in peers:
-        for core in range(2):
-            send(n_send, n_recv.at[slot], NR, p, core, recv=NR + s_me)
-    send(n_send, n_recv.at[slot], NR, me, 1 - tp, recv=NR + s_me)
-    n_recv[slot] = normed
+    await_recv(t_buf, TR, 1)
+    await_recv(ts_buf, TR + 1, 1)
+    await_recv(ps_recv, PS + 1, N_KV - 1)
+    await_recv(p_recv, PS, N_KV - 1)
+    for k in range(2):
+        stats_t = ps_recv[:, k].reshape(N_KV, LANES).T
+        peaks = stats_t[:PROPS]
+        bound = jnp.sum(stats_t[2 * PROPS : 2 * PROPS + 1], axis=1, keepdims=True)
+        tree_row = ts_buf[k]
+        tree_max = jnp.sum(jnp.where(diag == 0, tree_row, 0.0), axis=1, keepdims=True) - bound
+        tree_total = jnp.sum(jnp.where(diag == PROPS, tree_row, 0.0), axis=1, keepdims=True)
+        top = jnp.maximum(jnp.max(peaks, axis=1, keepdims=True), tree_max)
+        factors = jnp.exp(peaks - top)
+        tree_factor = jnp.exp(tree_max - top)
+        total = (
+            jnp.sum(factors * stats_t[PROPS : 2 * PROPS], axis=1, keepdims=True)
+            + tree_total * tree_factor
+        )
+        acc = [t_buf[k] * jnp.where(low8, tree_factor[:8], tree_factor[8:])] + [None] * 3
+        for i in range(N_KV):
+            factor = jnp.where(low8, factors[:8, i : i + 1], factors[8:, i : i + 1])
+            term = p_recv[i, k].astype(F32) * factor
+            acc[i % 4] = term if acc[i % 4] is None else acc[i % 4] + term
+        weighted = (acc[0] + acc[1]) + (acc[2] + acc[3])
+        attended = weighted / jnp.where(low8, total[:8], total[8:])
+        square = attended * attended
+        mean_low = jnp.sum(jnp.where(low8, square, 0.0), axis=1, keepdims=True) / DH
+        mean_high = jnp.sum(jnp.where(low8, 0.0, square), axis=1, keepdims=True) / DH
+        n_send[k] = (
+            attended * lax.rsqrt(jnp.where(low8, mean_low, mean_high) + EPSILON) * gain
+        ).astype(BF16)
+
+    slot = tp * HALF + pair
+    for o in NEAR:
+        for core in (tp, 1 - tp):
+            if o == (0, 0) and core is tp:
+                continue
+            send(n_send, n_recv.at[slot], NR, at(o), core, recv=NR + s_me % 2)
+    n_recv[slot] = n_send[...]
 
     @pl.when(s_me == 0)
     def _():
@@ -415,15 +462,17 @@
         kvn_ref[...] = jnp.zeros_like(kvn_ref)
 
     await_recv(wo_v, WO, 1)
-    for turn in (0, 1, 3, 2):
+    for turn in (0, 2, 1, 3):
         s = (s_me + turn) % SEQS
-        await_recv(n_recv, NR + s, 2 * HEADS if turn else 2 * HEADS - 1)
+        if turn < 2:
+            await_recv(n_recv, NR + s % 2, HALF if turn else HALF - 1)
         layer_sum = None
         for core in range(2):
             tiles = []
             for t in range(HEADS // 2):
-                m0 = n_recv[core * N_KV + s * HEADS + 2 * t].astype(F32)
-                m1 = n_recv[core * N_KV + s * HEADS + 2 * t + 1].astype(F32)
+                spot = core * HALF + s % 2 * HEADS + 2 * t
+                m0 = n_recv[spot, s // 2].astype(F32)
+                m1 = n_recv[spot + 1, s // 2].astype(F32)
                 tiles.append(
                     jnp.concatenate(
                         [jnp.where(low8, m0, swap(m1)), jnp.where(low8, swap(m0), m1)], axis=0
@@ -436,7 +485,10 @@
 
     await_send(q_send, 0, N_KV - 1)
     await_send(st_recv, 1, N_KV - 1)
-    await_send(kv_send, 2, N_KV - 1)
+    await_send(kvx_recv, 2, NX - 1)
+    await_send(kvz_recv, KVZ, NZ - 1)
+    await_send(t_buf, TR, 1)
+    await_send(ts_buf, TR + 1, 1)
     await_send(qn_recv, QN, N_KV - 1)
     await_send(wo_v, WO, 1)
 
@@ -452,9 +504,9 @@
     def _():
         await_send(kvn_recv, KVN, N_KV - FIRST_OWNER)
 
-    await_send(p_send, PS, N_KV - 1)
-    await_send(ps_send, PS + 1, N_KV - 1)
-    await_send(n_recv, NR, 2 * N_KV - 1)
+    await_send(p_recv, PS, N_KV - 1)
+    await_send(ps_recv, PS + 1, N_KV - 1)
+    await_send(n_recv, NR, N_KV - 1)
 
 
 def cache_kernel(
@@ -579,20 +631,24 @@
             pltpu.VMEM((N_KV, 8, LANES), F32),
             pltpu.VMEM((2 * HEADS, 1, LANES), F32),
             pltpu.VMEM((N_KV, 1, LANES), F32),
-            pltpu.VMEM((N_KV, PROPS, LANES), BF16),
-            pltpu.VMEM((N_KV, PROPS, LANES), BF16),
+            pltpu.VMEM((NX, NZ, PROPS, LANES), F32),
+            pltpu.VMEM((NX, NZ, PROPS, LANES), F32),
+            pltpu.VMEM((NZ, PROPS, LANES), F32),
+            pltpu.VMEM((NZ, PROPS, LANES), F32),
             pltpu.VMEM((8, LANES), BF16),
             pltpu.VMEM((N_KV, 8, LANES), BF16),
             pltpu.VMEM((PROPS, LANES), BF16),
             pltpu.VMEM((N_KV, PROPS, LANES), BF16),
             pltpu.VMEM((1, LANES), F32),
             pltpu.VMEM((HEADS, 1, LANES), F32),
-            pltpu.VMEM((N_KV, 8, LANES), F32),
-            pltpu.VMEM((N_KV, 8, LANES), F32),
-            pltpu.VMEM((N_KV, 1, LANES), F32),
-            pltpu.VMEM((N_KV, 1, LANES), F32),
-            pltpu.VMEM((8, LANES), BF16),
-            pltpu.VMEM((2 * N_KV, 8, LANES), BF16),
+            pltpu.VMEM((HALF, 2, 8, LANES), BF16),
+            pltpu.VMEM((N_KV, 2, 8, LANES), BF16),
+            pltpu.VMEM((HALF, 2, 1, LANES), F32),
+            pltpu.VMEM((N_KV, 2, 1, LANES), F32),
+            pltpu.VMEM((2, 8, LANES), F32),
+            pltpu.VMEM((2, 1, LANES), F32),
+            pltpu.VMEM((2, 8, LANES), BF16),
+            pltpu.VMEM((2 * HALF, 2, 8, LANES), BF16),
             pltpu.SemaphoreType.DMA((20,)),
             pltpu.SemaphoreType.DMA((24,)),
             pltpu.SemaphoreType.DMA((24,)),

time: 44.8 us -> 43 us (0.960)
  Pallas kernels: 44 us -> 42.2 us
    pallas_call x1, Pallas kernels: 41.4 us -> 39.6 us  [shards(): pl.pallas_call(layer_kernel, out_shape=(jax.ShapeDtypeStruct((SEQS, PROPS...]
where the time goes in v2:
time: 43 us
  Pallas kernels  42.2 us (98%)
  between operations  0.71 us (2%)
    pallas_call x1, Pallas kernels, shards(): pl.pallas_call(layer_kernel, out_shape=(jax.ShapeDtypeStruct((SEQS, PROPS...  39.6 us
    pallas_call x1, Pallas kernels, shards(): pl.pallas_call(cache_kernel, out_shape=(jax.ShapeDtypeStruct(layer_out.sh...  2.59 us

profile of v2, /device:TPU:1, one launch (start us, length us, event | category | flops | bytes accessed | tf_op | source)
XLA Modules:
  0.0 43.0 jit_solution(7641259546359576541)
XLA Ops:
  0.6 0.0 copy-start
  0.6 0.0 copy-start.1
  0.7 0.0 copy-start.2
  0.7 0.0 copy-start.3
  0.7 39.6 %layer.1 = (bf16[4,16,64]{2,1,0:T(8,128)(2,1)S(1)}, f32[4,8,16]{2,1,0:T(8,128)S(1)}, bf16[32,16,128]{2,1,0:T(8,128)(2,1)S(1)}) custom-call(bf16[4,16,64]{2,1,0:T(8,128)(2,1)} %tokens.1, f32[64]{0:T(128)} %norm_gain.1, bf16[64,512]{1,0:T(8,128)(2,1)} %w_query.1, bf16[64,512]{1,0:T(8,128)(2,1)} %w_key.1, bf16[64,512]{1,0:T(8,128)(2,1)} %w_value.1, ...), custom_call_target="tpu_custom_call" | custom-call | tf_op jit(solution)/shard_map/layer/pallas_call | solution.py:605
  40.3 0.0 copy-done
  40.3 0.0 copy-done.1
  40.4 0.0 copy-done.2
  40.4 0.0 copy-done.3
  40.4 2.6 %cache.1 = (bf16[4,16,64]{2,1,0:T(8,128)(2,1)}, bf16[4,512,512]{2,1,0:T(8,128)(2,1)}, bf16[4,512,512]{2,1,0:T(8,128)(2,1)}, f32[4,8,16]{2,1,0:T(8,128)}) custom-call(bf16[4,512,512]{2,1,0:T(8,128)(2,1)S(1)} %copy-done, bf16[4,512,512]{2,1,0:T(8,128)(2,1)S(1)} %copy-done.1, bf16[32,16,128]{2,1,0:T(8,128)(2,1)S(1)} %get-tuple-element.11.kvn, s32[4]{0:T(128)S(1)} %copy-done.2, ...), custom_call_target="tpu_custom_call" | custom-call | tf_op jit(solution)/shard_map/cache/pallas_call | solution.py:662
Async XLA Ops:
  0.6 39.7 %copy-start = (bf16[4,512,512]{2,1,0:T(8,128)(2,1)S(1)}, bf16[4,512,512]{2,1,0:T(8,128)(2,1)}, u32[]{:S(2)}) copy-start(bf16[4,512,512]{2,1,0:T(8,128)(2,1)} %key_cache.3) | copy-start | bytes 6291460
  0.6 39.7 %copy-start.1 = (bf16[4,512,512]{2,1,0:T(8,128)(2,1)S(1)}, bf16[4,512,512]{2,1,0:T(8,128)(2,1)}, u32[]{:S(2)}) copy-start(bf16[4,512,512]{2,1,0:T(8,128)(2,1)} %value_cache.3) | copy-start | bytes 6291460
  0.7 39.7 %copy-start.2 = (s32[4]{0:T(128)S(1)}, s32[4]{0:T(128)}, u32[]{:S(2)}) copy-start(s32[4]{0:T(128)} %lengths.3) | copy-start | bytes 52
  0.7 39.7 %copy-start.3 = (s32[4]{0:T(128)S(1)}, s32[4]{0:T(128)}, u32[]{:S(2)}) copy-start(s32[4]{0:T(128)} %accepted.3) | copy-start | bytes 52

commit v3 on v2

--- a/solution.py
+++ b/solution.py
@@ -23,6 +23,7 @@
 FEATS = D // N_KV
 LANES = 128
 FIRST_OWNER = 15341 // POS
+EARLY = 2 * NX
 CHUNK = 128
 QN, GL, KVN, PS, NR, WO, KVZ, TR = 3, 7, 8, 9, 11, 13, 14, 15
 
@@ -49,6 +50,27 @@
     return lax.dot_general(
         a, b, (dims, ((), ())), preferred_element_type=F32, precision=precision
     )
+
+
+def early_kernel(key_cache, value_cache, new_keys, new_values, token, k_v, v_v, rsem, wsem):
+    token[...] = jnp.zeros_like(token)
+
+    @pl.when(lax.axis_index("kv") < EARLY)
+    def _():
+        reads, writes = [], []
+        for s in range(SEQS):
+            for i, (src, buf, dst) in enumerate(
+                ((key_cache, k_v, new_keys), (value_cache, v_v, new_values))
+            ):
+                reads.append(pltpu.make_async_copy(src.at[s], buf.at[s], rsem.at[2 * s + i]))
+                writes.append(pltpu.make_async_copy(buf.at[s], dst.at[s], wsem.at[2 * s + i]))
+        for copy in reads:
+            copy.start()
+        for read, write in zip(reads, writes):
+            read.wait()
+            write.start()
+        for copy in writes:
+            copy.wait()
 
 
 def layer_kernel(
@@ -69,6 +91,7 @@
     lengths,
     accepted,
     parents,
+    token,
     out_ref,
     gates_ref,
     kvn_ref,
@@ -513,17 +536,22 @@
     key_cache,
     value_cache,
     kvn,
-    lengths,
-    accepted,
+    lengths_in,
+    accepted_in,
     layer_in,
     gates_in,
+    keys_in,
+    values_in,
     layer_out,
     new_keys,
     new_values,
     gates_out,
     k_v,
     v_v,
+    lengths,
+    accepted,
     sem,
+    small_sem,
 ):
     me = lax.axis_index("kv")
     sides = ((key_cache, k_v, new_keys), (value_cache, v_v, new_values))
@@ -531,6 +559,8 @@
         pltpu.make_async_copy(layer_in, layer_out, sem.at[0]),
         pltpu.make_async_copy(gates_in, gates_out, sem.at[1]),
     ]
+    for copy in ends:
+        copy.start()
 
     def write(s, c, side, patched):
         src, buf, dst = sides[side]
@@ -539,22 +569,37 @@
             (buf if patched else src).at[s, rows], dst.at[s, rows], sem.at[2 + s]
         )
 
-    for s in range(SEQS):
-        offset = lengths[s] + accepted[s] - me * POS
-        for c in range(POS // CHUNK):
-            clear = (offset >= (c + 1) * CHUNK) | (offset + PROPS <= c * CHUNK)
-
-            @pl.when(clear)
-            def _():
-                for side in range(2):
-                    write(s, c, side, False).start()
-
-    for copy in ends:
-        copy.start()
+    def whole(s, src, dst):
+        return pltpu.make_async_copy(src.at[s], dst.at[s], sem.at[2 + s])
+
+    @pl.when((me >= EARLY) & (me < FIRST_OWNER))
+    def _():
+        for s in range(SEQS):
+            for src, _, dst in sides:
+                whole(s, src, dst).start()
+
     low = iota((CHUNK, LANES), 1) < DH
 
     @pl.when(me >= FIRST_OWNER)
     def _():
+        small = [
+            pltpu.make_async_copy(lengths_in, lengths, small_sem.at[0]),
+            pltpu.make_async_copy(accepted_in, accepted, small_sem.at[1]),
+        ]
+        for copy in small:
+            copy.start()
+        for copy in small:
+            copy.wait()
+        for s in range(SEQS):
+            offset = lengths[s] + accepted[s] - me * POS
+            for c in range(POS // CHUNK):
+                clear = (offset >= (c + 1) * CHUNK) | (offset + PROPS <= c * CHUNK)
+
+                @pl.when(clear)
+                def _():
+                    for side in range(2):
+                        write(s, c, side, False).start()
+
         for s in range(SEQS):
             offset = lengths[s] + accepted[s] - me * POS
 
@@ -587,9 +632,12 @@
                 def _():
                     patch(last)
 
-    for s in range(SEQS):
-        for src, _, dst in sides:
-            pltpu.make_async_copy(src.at[s], dst.at[s], sem.at[2 + s]).wait()
+    @pl.when(me >= EARLY)
+    def _():
+        for s in range(SEQS):
+            for src, _, dst in sides:
+                whole(s, src, dst).wait()
+
     for copy in ends:
         copy.wait()
 
@@ -597,11 +645,29 @@
 def shards(*args):
     hbm = pl.BlockSpec(memory_space=pltpu.HBM)
     vmem = pl.BlockSpec(memory_space=pltpu.VMEM)
-    smem = pl.BlockSpec(memory_space=pltpu.SMEM)
     operands = list(args)
     operands[5] = operands[5].T
     operands[10] = operands[10].T
     operands = [pltpu.with_memory_space_constraint(a, pltpu.HBM) for a in operands]
+    key_cache, value_cache = args[11], args[12]
+    early_keys, early_values, token = pl.pallas_call(
+        early_kernel,
+        out_shape=(
+            jax.ShapeDtypeStruct(key_cache.shape, BF16),
+            jax.ShapeDtypeStruct(value_cache.shape, BF16),
+            jax.ShapeDtypeStruct((8, LANES), F32),
+        ),
+        in_specs=[hbm, hbm],
+        out_specs=(hbm, hbm, vmem),
+        scratch_shapes=[
+            pltpu.VMEM((SEQS, POS, WIDTH), BF16),
+            pltpu.VMEM((SEQS, POS, WIDTH), BF16),
+            pltpu.SemaphoreType.DMA((2 * SEQS,)),
+            pltpu.SemaphoreType.DMA((2 * SEQS,)),
+        ],
+        compiler_params=pltpu.CompilerParams(vmem_limit_bytes=16 * 2**20),
+        name="early",
+    )(operands[11], operands[12])
     layer_out, gates, kvn = pl.pallas_call(
         layer_kernel,
         out_shape=(
@@ -609,7 +675,7 @@
             jax.ShapeDtypeStruct((SEQS, HEADS, PROPS), F32),
             jax.ShapeDtypeStruct((N_KV, PROPS, LANES), BF16),
         ),
-        in_specs=[hbm] * len(operands),
+        in_specs=[hbm] * len(operands) + [pl.BlockSpec(memory_space=pl.ANY)],
         out_specs=(vmem, vmem, vmem),
         scratch_shapes=[
             pltpu.VMEM((SEQS, PROPS, FEATS), BF16),
@@ -657,8 +723,7 @@
             collective_id=0, has_side_effects=True, vmem_limit_bytes=24 * 2**20
         ),
         name="layer",
-    )(*operands)
-    key_cache, value_cache, lengths, accepted = args[11], args[12], args[14], args[15]
+    )(*operands, token)
     layer_out, new_keys, new_values, gates = pl.pallas_call(
         cache_kernel,
         out_shape=(
@@ -667,16 +732,30 @@
             jax.ShapeDtypeStruct(value_cache.shape, BF16),
             jax.ShapeDtypeStruct(gates.shape, F32),
         ),
-        in_specs=[vmem, vmem, vmem, smem, smem, vmem, vmem],
+        in_specs=[vmem, vmem, vmem, hbm, hbm, vmem, vmem, hbm, hbm],
         out_specs=(hbm, hbm, hbm, hbm),
+        input_output_aliases={7: 1, 8: 2},
         scratch_shapes=[
             pltpu.VMEM((SEQS, POS, WIDTH), BF16),
             pltpu.VMEM((SEQS, POS, WIDTH), BF16),
+            pltpu.SMEM((SEQS,), jnp.int32),
+            pltpu.SMEM((SEQS,), jnp.int32),
             pltpu.SemaphoreType.DMA((2 + SEQS,)),
+            pltpu.SemaphoreType.DMA((2,)),
         ],
         compiler_params=pltpu.CompilerParams(vmem_limit_bytes=16 * 2**20),
         name="cache",
-    )(key_cache, value_cache, kvn, lengths, accepted, layer_out, gates)
+    )(
+        key_cache,
+        value_cache,
+        kvn,
+        operands[14],
+        operands[15],
+        layer_out,
+        gates,
+        early_keys,
+        early_values,
+    )
     return layer_out, new_keys, new_values, jnp.transpose(gates, (0, 2, 1))
 
 

time: 43 us -> 41.2 us (0.958)
  Pallas kernels: 42.2 us -> 40.4 us
    pallas_call x0 -> x1, Pallas kernels: none -> 3.59 us  [shards(): pl.pallas_call(early_kernel, out_shape=(jax.ShapeDtypeStruct(key_cache.sh...]
    pallas_call x1, Pallas kernels: 39.6 us -> 36.1 us  [shards(): pl.pallas_call(layer_kernel, out_shape=(jax.ShapeDtypeStruct((SEQS, PROPS...]
    pallas_call x1, Pallas kernels: 2.59 us -> 0.69 us  [shards(): pl.pallas_call(cache_kernel, out_shape=(jax.ShapeDtypeStruct(layer_out.sh...]
where the time goes in v3:
time: 41.2 us; the launch traced here: 41.1 us
  Pallas kernels  40.4 us (98%)
  between operations  0.68 us (2%)
    pallas_call x1, Pallas kernels, shards(): pl.pallas_call(layer_kernel, out_shape=(jax.ShapeDtypeStruct((SEQS, PROPS...  36.1 us
    pallas_call x1, Pallas kernels, shards(): pl.pallas_call(early_kernel, out_shape=(jax.ShapeDtypeStruct(key_cache.sh...  3.59 us

profile of v3, /device:TPU:1, one launch (start us, length us, event | category | flops | bytes accessed | tf_op | source)
XLA Modules:
  0.0 41.1 jit_solution(10354883435722970427)
XLA Ops:
  0.6 3.6 %early.1 = (bf16[4,512,512]{2,1,0:T(8,128)(2,1)}, bf16[4,512,512]{2,1,0:T(8,128)(2,1)}, f32[8,128]{1,0:T(8,128)S(1)}) custom-call(bf16[4,512,512]{2,1,0:T(8,128)(2,1)} %key_cache.5, bf16[4,512,512]{2,1,0:T(8,128)(2,1)} %value_cache.5), custom_call_target="tpu_custom_call" | custom-call | tf_op jit(solution)/shard_map/early/pallas_call | solution.py:653
  4.2 0.0 copy-start
  4.2 0.0 copy-start.1
  4.2 36.1 %layer.1 = (bf16[4,16,64]{2,1,0:T(8,128)(2,1)S(1)}, f32[4,8,16]{2,1,0:T(8,128)S(1)}, bf16[32,16,128]{2,1,0:T(8,128)(2,1)S(1)}) custom-call(bf16[4,16,64]{2,1,0:T(8,128)(2,1)} %tokens.1, f32[64]{0:T(128)} %norm_gain.1, bf16[64,512]{1,0:T(8,128)(2,1)} %w_query.1, bf16[64,512]{1,0:T(8,128)(2,1)} %w_key.1, bf16[64,512]{1,0:T(8,128)(2,1)} %w_value.1, ...), custom_call_target="tpu_custom_call" | custom-call | tf_op jit(solution)/shard_map/layer/pallas_call | solution.py:671
  40.4 0.0 copy-done
  40.4 0.0 copy-done.1
  40.4 0.7 %cache.1 = (bf16[4,16,64]{2,1,0:T(8,128)(2,1)}, bf16[4,512,512]{2,1,0:T(8,128)(2,1)}, bf16[4,512,512]{2,1,0:T(8,128)(2,1)}, f32[4,8,16]{2,1,0:T(8,128)}) custom-call(bf16[4,512,512]{2,1,0:T(8,128)(2,1)S(1)} %copy-done, bf16[4,512,512]{2,1,0:T(8,128)(2,1)S(1)} %copy-done.1, ...), custom_call_target="tpu_custom_call", output_to_operand_aliasing={{1}: (7, {}), {2}: (8, {})} | custom-call | tf_op jit(solution)/shard_map/cache/pallas_call | solution.py:727
Async XLA Ops:
  4.2 36.1 %copy-start = (bf16[4,512,512]{2,1,0:T(8,128)(2,1)S(1)}, bf16[4,512,512]{2,1,0:T(8,128)(2,1)}, u32[]{:S(2)}) copy-start(bf16[4,512,512]{2,1,0:T(8,128)(2,1)} %key_cache.5) | copy-start | bytes 6291460
  4.2 36.1 %copy-start.1 = (bf16[4,512,512]{2,1,0:T(8,128)(2,1)S(1)}, bf16[4,512,512]{2,1,0:T(8,128)(2,1)}, u32[]{:S(2)}) copy-start(bf16[4,512,512]{2,1,0:T(8,128)(2,1)} %value_cache.5) | copy-start | bytes 6291460

commit v4 on v3

--- a/solution.py
+++ b/solution.py
@@ -132,6 +132,8 @@
     ts_buf,
     n_send,
     n_recv,
+    t_send,
+    ts_send,
     load_sem,
     ssem,
     rsem,
@@ -145,7 +147,10 @@
 
     peers = [at(o) for o in OFFSETS]
     s_me, h_me = me // HEADS, me % HEADS
-    pair, half = me % HALF, me // HALF
+    half = me // HALF
+    pair = (mz + 2) % (NZ // 2) * NX + (mx + NX - 1) % NX
+    group = pair // HEADS
+    other_half = (me + HALF) % N_KV
 
     loads = []
 
@@ -321,7 +326,7 @@
         copy.wait()
     pos = iota((1, POS), 1) + me * POS
     diag = iota((PROPS, LANES), 1) - iota((PROPS, LANES), 0)
-    corner = (iota((PROPS, LANES), 0) == 0) & (iota((PROPS, LANES), 1) == 2 * PROPS)
+    corner = jnp.where(iota((PROPS, LANES), 0) == 0, iota((PROPS, LANES), 1) - 2 * PROPS, -1)
     for turn in (0, 1, 3, 2):
         s = (s_me + turn) % SEQS
         await_recv(qn_recv, QN + s, HEADS if turn else HEADS - 1)
@@ -364,20 +369,27 @@
             for odd in range(2):
                 rows_at = slice(odd * PROPS, (odd + 1) * PROPS)
                 head = 2 * t + odd
-                tile = jnp.where(diag == 0, peak[rows_at], 0.0)
-                tile = jnp.where(diag == PROPS, total[rows_at], tile)
-                tile = jnp.where(corner, bound[head : head + 1], tile)
-                ps_send[s % 2 * HEADS + head, s // 2] = jnp.sum(tile, axis=0, keepdims=True)
+                shift = s // 2 * DH
+                tile = jnp.where(diag == shift, peak[rows_at], 0.0)
+                tile = jnp.where(diag == PROPS + shift, total[rows_at], tile)
+                tile = jnp.where(corner == shift, bound[head : head + 1], tile)
+                row = jnp.sum(tile, axis=0, keepdims=True)
+                if turn in (2, 3):
+                    row = row + ps_send[s % 2 * HEADS + head]
+                ps_send[s % 2 * HEADS + head] = row
         if turn not in (2, 3):
             continue
-        for side in (s, (s + 2) % SEQS):
-            for j in range(HEADS):
-                if turn == 2 and side is not s and j == 0:
-                    continue
-                head = (h_me + j) % HEADS
-                target = side * HEADS + head
-                send(p_send.at[s % 2 * HEADS + head], p_recv.at[me], PS, target)
-                send(ps_send.at[s % 2 * HEADS + head], ps_recv.at[me], PS + 1, target)
+        for j in range(HEADS):
+            head = (pair + j) % HEADS
+            at_pair = s % 2 * HEADS + head
+            target = (at_pair // NX + 2) % (NZ // 2) * NX + (head + 1) % NX
+            if turn == 3 and j == 0:
+                targets = (other_half,)
+            else:
+                targets = (target, target + HALF)
+            for target in targets:
+                send(p_send.at[at_pair], p_recv.at[me], PS, target)
+                send(ps_send.at[at_pair], ps_recv.at[me], PS + 1, target)
     p_recv[me] = p_send[pair]
     ps_recv[me] = ps_send[pair]
 
@@ -408,27 +420,28 @@
     tree = dot(q_rows, kv_new, ((1,), (1,))) * DH**-0.5 - path_row
     tree_live = ancestors > 0.5
     tree = jnp.where(tree_live, tree, MASKED)
-    mirror = (me + HALF) % N_KV
     tree_max = jnp.max(tree, axis=1, keepdims=True)
     tree_weights = jnp.where(tree_live, jnp.exp(tree - tree_max), 0.0)
     tree_total = jnp.sum(tree_weights, axis=1, keepdims=True)
     tree_sum = dot(tree_weights.astype(BF16), kv_new, ((1,), (0,)))
     tree_packed = jnp.where(low8, swap(tree_sum[:8]), tree_sum[8:])
-    t_buf[half] = tree_packed
+    t_send[...] = tree_packed
     tile = jnp.where(diag == 0, tree_max, 0.0)
     tile = jnp.where(diag == PROPS, tree_total, tile)
-    ts_buf[half] = jnp.sum(tile, axis=0, keepdims=True)
-    send(t_buf.at[half], t_buf.at[half], TR, mirror)
-    send(ts_buf.at[half], ts_buf.at[half], TR + 1, mirror)
+    ts_send[...] = jnp.sum(tile, axis=0, keepdims=True)
+    for dz in (2, NZ - 2):
+        send(t_send, t_buf.at[half], TR, at((dz, 1)))
+        send(ts_send, ts_buf.at[half], TR + 1, at((dz, 1)))
 
     gain = hg_v[...].reshape(1, DH)
     gain = jnp.concatenate([gain, gain], axis=1)
-    await_recv(t_buf, TR, 1)
-    await_recv(ts_buf, TR + 1, 1)
+    await_recv(t_buf, TR, 2)
+    await_recv(ts_buf, TR + 1, 2)
     await_recv(ps_recv, PS + 1, N_KV - 1)
     await_recv(p_recv, PS, N_KV - 1)
+    both_t = ps_recv[...].reshape(N_KV, LANES).T
     for k in range(2):
-        stats_t = ps_recv[:, k].reshape(N_KV, LANES).T
+        stats_t = both_t[k * DH : (k + 1) * DH]
         peaks = stats_t[:PROPS]
         bound = jnp.sum(stats_t[2 * PROPS : 2 * PROPS + 1], axis=1, keepdims=True)
         tree_row = ts_buf[k]
@@ -460,7 +473,7 @@
         for core in (tp, 1 - tp):
             if o == (0, 0) and core is tp:
                 continue
-            send(n_send, n_recv.at[slot], NR, at(o), core, recv=NR + s_me % 2)
+            send(n_send, n_recv.at[slot], NR, at(o), core, recv=NR + group)
     n_recv[slot] = n_send[...]
 
     @pl.when(s_me == 0)
@@ -486,7 +499,7 @@
 
     await_recv(wo_v, WO, 1)
     for turn in (0, 2, 1, 3):
-        s = (s_me + turn) % SEQS
+        s = (group + turn) % SEQS
         if turn < 2:
             await_recv(n_recv, NR + s % 2, HALF if turn else HALF - 1)
         layer_sum = None
@@ -510,8 +523,8 @@
     await_send(st_recv, 1, N_KV - 1)
     await_send(kvx_recv, 2, NX - 1)
     await_send(kvz_recv, KVZ, NZ - 1)
-    await_send(t_buf, TR, 1)
-    await_send(ts_buf, TR + 1, 1)
+    await_send(t_buf, TR, 2)
+    await_send(ts_buf, TR + 1, 2)
     await_send(qn_recv, QN, N_KV - 1)
     await_send(wo_v, WO, 1)
 
@@ -709,12 +722,14 @@
             pltpu.VMEM((HEADS, 1, LANES), F32),
             pltpu.VMEM((HALF, 2, 8, LANES), BF16),
             pltpu.VMEM((N_KV, 2, 8, LANES), BF16),
-            pltpu.VMEM((HALF, 2, 1, LANES), F32),
-            pltpu.VMEM((N_KV, 2, 1, LANES), F32),
+            pltpu.VMEM((HALF, 1, LANES), F32),
+            pltpu.VMEM((N_KV, 1, LANES), F32),
             pltpu.VMEM((2, 8, LANES), F32),
             pltpu.VMEM((2, 1, LANES), F32),
             pltpu.VMEM((2, 8, LANES), BF16),
             pltpu.VMEM((2 * HALF, 2, 8, LANES), BF16),
+            pltpu.VMEM((8, LANES), F32),
+            pltpu.VMEM((1, LANES), F32),
             pltpu.SemaphoreType.DMA((20,)),
             pltpu.SemaphoreType.DMA((24,)),
             pltpu.SemaphoreType.DMA((24,)),

time: 41.2 us -> 40.8 us (level)
  no operation moved by 1% of the time
where the time goes in v4:
time: 40.8 us
  Pallas kernels  40.1 us (98%)
  between operations  0.68 us (2%)
    pallas_call x1, Pallas kernels, shards(): pl.pallas_call(layer_kernel, out_shape=(jax.ShapeDtypeStruct((SEQS, PROPS...  35.8 us
    pallas_call x1, Pallas kernels, shards(): pl.pallas_call(early_kernel, out_shape=(jax.ShapeDtypeStruct(key_cache.sh...  3.59 us

profile of v4, /device:TPU:1, one launch (start us, length us, event | category | flops | bytes accessed | tf_op | source)
XLA Modules:
  0.0 40.8 jit_solution(12104359462509442723)
XLA Ops:
  0.6 3.6 %early.1 = (bf16[4,512,512]{2,1,0:T(8,128)(2,1)}, bf16[4,512,512]{2,1,0:T(8,128)(2,1)}, f32[8,128]{1,0:T(8,128)S(1)}) custom-call(bf16[4,512,512]{2,1,0:T(8,128)(2,1)} %key_cache.5, bf16[4,512,512]{2,1,0:T(8,128)(2,1)} %value_cache.5), custom_call_target="tpu_custom_call" | custom-call | tf_op jit(solution)/shard_map/early/pallas_call | solution.py:666
  4.2 0.0 copy-start
  4.2 0.0 copy-start.1
  4.2 35.8 %layer.1 = (bf16[4,16,64]{2,1,0:T(8,128)(2,1)S(1)}, f32[4,8,16]{2,1,0:T(8,128)S(1)}, bf16[32,16,128]{2,1,0:T(8,128)(2,1)S(1)}) custom-call(bf16[4,16,64]{2,1,0:T(8,128)(2,1)} %tokens.1, f32[64]{0:T(128)} %norm_gain.1, bf16[64,512]{1,0:T(8,128)(2,1)} %w_query.1, bf16[64,512]{1,0:T(8,128)(2,1)} %w_key.1, bf16[64,512]{1,0:T(8,128)(2,1)} %w_value.1, ...), custom_call_target="tpu_custom_call" | custom-call | tf_op jit(solution)/shard_map/layer/pallas_call | solution.py:684
  40.0 0.0 copy-done
  40.1 0.0 copy-done.1
  40.1 0.7 %cache.1 = (bf16[4,16,64]{2,1,0:T(8,128)(2,1)}, bf16[4,512,512]{2,1,0:T(8,128)(2,1)}, bf16[4,512,512]{2,1,0:T(8,128)(2,1)}, f32[4,8,16]{2,1,0:T(8,128)}) custom-call(bf16[4,512,512]{2,1,0:T(8,128)(2,1)S(1)} %copy-done, bf16[4,512,512]{2,1,0:T(8,128)(2,1)S(1)} %copy-done.1, ...), custom_call_target="tpu_custom_call", output_to_operand_aliasing={{1}: (7, {}), {2}: (8, {})} | custom-call | tf_op jit(solution)/shard_map/cache/pallas_call | solution.py:742
Async XLA Ops:
  4.2 35.8 %copy-start = (bf16[4,512,512]{2,1,0:T(8,128)(2,1)S(1)}, bf16[4,512,512]{2,1,0:T(8,128)(2,1)}, u32[]{:S(2)}) copy-start(bf16[4,512,512]{2,1,0:T(8,128)(2,1)} %key_cache.5) | copy-start | bytes 6291460
  4.2 35.8 %copy-start.1 = (bf16[4,512,512]{2,1,0:T(8,128)(2,1)S(1)}, bf16[4,512,512]{2,1,0:T(8,128)(2,1)}, u32[]{:S(2)}) copy-start(bf16[4,512,512]{2,1,0:T(8,128)(2,1)} %value_cache.5) | copy-start | bytes 6291460
